TPU v7x, 32 devices: a whole 2x2x4 slice. The times are simulated.
32 devices in a mesh: ep: 16 (over z, x, core), tp: 2 (over y).
Axes of the slice: x: 2, y: 2, z: 4, core: 2. Of those that a mesh axis runs over, the one named last changes fastest.
Arguments:
- tokens: bfloat16 [512, 2048], P('ep'), may hold values from -6 to 6
- norm_gain_attn: float32 [2048], replicated, may hold values from 0.1 to 1.9
- w_query: bfloat16 [2048, 2048], P('ep', 'tp'), may hold values from -0.125 to 0.125
- w_key: bfloat16 [2048, 256], P('ep', 'tp'), may hold values from -0.125 to 0.125
- w_value: bfloat16 [2048, 256], P('ep', 'tp'), may hold values from -0.125 to 0.125
- w_forget: bfloat16 [2048, 32], P(None, 'tp'), may hold values from -0.125 to 0.125
- forget_bias: float32 [32], P('tp'), may hold values from -1 to 3
- cache_keys: bfloat16 [512, 256, 1024], P('ep', 'tp'), may hold values from -64 to 64
- cache_values: bfloat16 [512, 256, 1024], P('ep', 'tp'), may hold values from -6 to 6
- cache_logcum: float32 [512, 32, 1024], P('ep', 'tp'), may hold values from -2048 to 0, as said below
- lengths: int32 [512], P('ep'), may hold values from 1 to 1023, as said below
- w_out: bfloat16 [2048, 2048], P('tp'), may hold values from -0.125 to 0.125
- norm_gain_mix: float32 [2048], replicated, may hold values from 0.1 to 1.9
- norm_gain_ffn: float32 [2048], replicated, may hold values from 0.1 to 1.9
- expert_gate: bfloat16 [2048, 16384], P(None, ('ep', 'tp')), may hold values from -0.125 to 0.125
- expert_up: bfloat16 [2048, 16384], P(None, ('ep', 'tp')), may hold values from -0.125 to 0.125
- expert_down: bfloat16 [16384, 2048], P(('ep', 'tp')), may hold values from -0.09375 to 0.09375
- routes: int32 [512, 2], P('ep'), may hold values from 0 to 3, all different within a row; in each aligned block of 32 rows (0 to 31, 32 to 63, ...) at most 32 rows name the same one
- route_weights: float32 [512, 2], P('ep'), may hold values from 0.2 to 1
Outputs:
- layer_out: bfloat16 [512, 2048], P('ep', 'tp')
- new_keys: bfloat16 [512, 256], P('ep', 'tp')
- new_values: bfloat16 [512, 256], P('ep', 'tp')
- new_log_gate: float32 [512, 32], P('ep', 'tp')
Inputs may be any that keep to these rules, and one draw needn't show every extreme that they name: `routes`: each row names 2 different experts. Within the rows of one index of ep no expert is named by more than 32 rows, and in every draw some expert is named by exactly 32 rows of some index. `lengths`: some sequence has 1023 cached positions in every draw. `cache_logcum`: never rising along positions (the last dimension).
All inputs are finite; a program needn't handle non-finite values.
Results may differ from a plain program's by a relative error of at most 0.013.
Values may be sent and summed in bfloat16 or wider, within the bound.
A program may use at most 64 MiB of HBM per device.

v0:
```python
import functools

import jax
import jax.numpy as jnp
from jax import lax
from jax.experimental import pallas as pl
from jax.experimental.pallas import tpu as pltpu
from jax.sharding import PartitionSpec as P

HEAD_TOTAL = 32
KV_HEADS = 4
HEAD_DIM = 64
SPAN = 4
TOP = 2


EPSILON = 1e-06
MASKED = -1e30


def rms_scaled(field, gain_vector):
    return (
        field * lax.rsqrt(jnp.mean(field * field, axis=-1, keepdims=True) + EPSILON) * gain_vector
    )


VMEM = pltpu.VMEM
MESH = pl.DeviceIdType.MESH
BF16 = jnp.bfloat16
F32 = jnp.float32


def bit_count(devices):
    return devices.bit_length() - 1


def reversed_bits(place, bits):
    return sum(((place >> b) & 1) << (bits - 1 - b) for b in range(bits))


def flipped(me, mask, bits):
    other = me
    for b in range(bits):
        if (mask >> b) & 1:
            other = other + (1 - 2 * ((me // (1 << b)) % 2)) * (1 << b)
    return other


def greet(partners):
    barrier = pltpu.get_barrier_semaphore()
    for partner in partners:
        pl.semaphore_signal(barrier, inc=1, device_id=partner, device_id_type=MESH)
    pl.semaphore_wait(barrier, len(partners))


def remote(src, dst, send_sem, recv_sem, partner):
    return pltpu.make_async_remote_copy(
        src_ref=src,
        dst_ref=dst,
        send_sem=send_sem,
        recv_sem=recv_sem,
        device_id=partner,
        device_id_type=MESH,
    )


def add_into(acc, got, low, high, shift, cols):
    acc[low:high, :, cols] = (
        acc[low:high, :, cols].astype(F32) + got[low + shift : high + shift, :, cols].astype(F32)
    ).astype(BF16)


def project_kernel(
    devices, chunk, x_ref, wq_ref, wk_ref, wv_ref, out_ref, xs, acc, got, xsend, xrecv, send, recv
):
    bits = bit_count(devices)
    me, tp = lax.axis_index("ep"), lax.axis_index("tp")
    rows, depth = xs.shape[1], xs.shape[2]
    total = acc.shape[2]
    greet([(flipped(me, m, bits), tp) for m in range(1, devices)])
    moves = {}
    for s in range(devices - 1, 0, -1):
        other = flipped(me, reversed_bits(s, bits), bits)
        cols = pl.ds(pl.multiple_of(other * depth, depth), depth)
        moves[s] = remote(x_ref.at[:, cols], xs.at[s], xsend.at[s], xrecv.at[s], (other, tp))
        moves[s].start()
    own = pltpu.make_async_copy(
        x_ref.at[:, pl.ds(pl.multiple_of(me * depth, depth), depth)], xs.at[0], xrecv.at[0]
    )
    own.start()
    own.wait()
    half = devices // 2
    copies = {}

    def exchange(step, c):
        n = half >> step
        cols = pl.ds(c * chunk, chunk)
        other = flipped(me, 1 << step, bits)
        copies[step, c] = remote(
            acc.at[n : 2 * n, :, cols],
            got.at[n : 2 * n, :, cols],
            send.at[step, c],
            recv.at[step, c],
            (other, tp),
        )
        copies[step, c].start()

    def multiply(low, high):
        left = xs[low:high].reshape((high - low) * rows, depth)
        start = 0
        for w_ref in (wq_ref, wk_ref, wv_ref):
            width = w_ref.shape[1]
            part = jnp.dot(left, w_ref[...], preferred_element_type=F32)
            acc[low:high, :, start : start + width] = part.astype(BF16).reshape(
                high - low, rows, width
            )
            start += width

    chunks = total // chunk
    for s in range(devices - 1, half - 1, -1):
        moves[s].wait_recv()
    multiply(half, devices)
    for c in range(chunks):
        exchange(0, c)
    for s in range(half - 1, 0, -1):
        moves[s].wait_recv()
    multiply(0, half)
    for step in range(bits):
        n = half >> step
        for c in range(chunks):
            copies[step, c].wait_recv()
            cols = slice(c * chunk, (c + 1) * chunk)
            if step + 1 < bits:
                add_into(acc, got, n // 2, n, n, cols)
                exchange(step + 1, c)
                add_into(acc, got, 0, n // 2, n, cols)
            else:
                out_ref[:, cols] = (
                    acc[0, :, cols].astype(F32) + got[1, :, cols].astype(F32)
                ).astype(BF16)
    for s in moves:
        moves[s].wait_send()
    for key in copies:
        copies[key].wait_send()


def dispatch_kernel(
    devices,
    chunks,
    part_ref,
    tok_ref,
    gmix_ref,
    gffn_ref,
    wts_ref,
    res_ref,
    all_ref,
    wall_ref,
    theirs,
    tsend,
    trecv,
    send,
    recv,
    wsend,
    wrecv,
):
    bits = bit_count(devices)
    me, tp = lax.axis_index("ep"), lax.axis_index("tp")
    other_tp = (me, 1 - tp)
    partners = [(flipped(me, 1 << b, bits), tp) for b in range(bits)]
    greet(partners + [other_tp])
    swap = remote(part_ref, theirs, tsend.at[0], trecv.at[0], other_tp)
    swap.start()
    wall_ref[0] = wts_ref[...]
    swap.wait_recv()
    mix = part_ref[...].astype(F32) + theirs[...].astype(F32)
    mixed_res = tok_ref[...].astype(F32) + rms_scaled(mix, gmix_ref[...])
    res_ref[...] = mixed_res
    all_ref[0] = rms_scaled(mixed_res, gffn_ref[...]).astype(BF16)
    width = all_ref.shape[2] // chunks
    copies = {}
    shared = chunks - 2
    half = 1 << (bits - 1)

    def columns(c):
        piece = chunks - 2 + tp if c == shared else c
        return pl.ds(pl.multiple_of(piece * width, width), width)

    def exchange(step, c, cols=None):
        n = 1 << step
        partner = partners[bits - 1 - step]
        if c < chunks:
            cols = columns(c) if cols is None else cols
            move = remote(
                all_ref.at[0:n, :, cols],
                all_ref.at[n : 2 * n, :, cols],
                send.at[step, c],
                recv.at[step, c],
                partner,
            )
        else:
            move = remote(
                wall_ref.at[0:n], wall_ref.at[n : 2 * n], wsend.at[step], wrecv.at[step], partner
            )
        copies[step, c] = move
        move.start()

    order = [shared] + list(range(shared)) + [chunks]
    for step in range(bits - 1):
        for c in order:
            if step:
                copies[step - 1, c].wait_recv()
            exchange(step, c)
    copies[bits - 2, shared].wait_recv()
    across = remote(
        all_ref.at[1:half, :, columns(shared)],
        all_ref.at[1:half, :, columns(shared)],
        tsend.at[1],
        trecv.at[1],
        other_tp,
    )
    across.start()
    exchange(bits - 1, shared)
    for c in order[1:]:
        copies[bits - 2, c].wait_recv()
        exchange(bits - 1, c)
    across.wait_recv()
    theirs_cols = pl.ds(pl.multiple_of((chunks - 1 - tp) * width, width), width)
    exchange(bits - 1, chunks - 1, theirs_cols)
    for c in order + [chunks - 1]:
        copies[bits - 1, c].wait_recv()
    swap.wait_send()
    across.wait_send()
    for key in copies:
        copies[key].wait_send()


def combine_kernel(devices, chunk, acc_in, out_ref, acc, got0, got1, got, send, recv):
    bits = bit_count(devices)
    me, tp = lax.axis_index("ep"), lax.axis_index("tp")
    partners = [(flipped(me, 1 << b, bits), tp) for b in range(bits)]
    other_tp = (me, 1 - tp)
    greet(partners + [other_tp])
    half = devices // 2
    share = acc.shape[2]
    chunks = share // chunk
    copies = {}

    def ds(side, c):
        return pl.ds(pl.multiple_of(side * share + c * chunk, 128), chunk)

    for side in range(2):
        for c in range(chunks):
            where = ds(1 - tp, c) if side == 0 else ds(tp, c)
            copies[0, side, c] = remote(
                acc_in.at[half:devices, :, where],
                got0.at[side, :, :, pl.ds(c * chunk, chunk)],
                send.at[side, c],
                recv.at[side, c],
                partners[0],
            )
            copies[0, side, c].start()
    outgoing = got1.at[0]
    incoming = got1.at[1]
    for c in range(chunks):
        cols = slice(c * chunk, (c + 1) * chunk)
        copies[0, 0, c].wait_recv()
        outgoing[:, :, cols] = (
            acc_in[0:half, :, ds(1 - tp, c)].astype(F32) + got0[0, :, :, cols].astype(F32)
        ).astype(BF16)
        copies[1, 0, c] = remote(
            outgoing.at[:, :, pl.ds(c * chunk, chunk)],
            incoming.at[:, :, pl.ds(c * chunk, chunk)],
            send.at[2, c],
            recv.at[2, c],
            other_tp,
        )
        copies[1, 0, c].start()
    for c in range(chunks):
        cols = slice(c * chunk, (c + 1) * chunk)
        copies[0, 1, c].wait_recv()
        acc[:, :, cols] = (
            acc_in[0:half, :, ds(tp, c)].astype(F32) + got0[1, :, :, cols].astype(F32)
        ).astype(BF16)

    def exchange(step, c):
        n = half >> step
        copies[step + 1, 0, c] = remote(
            acc.at[n : 2 * n, :, pl.ds(c * chunk, chunk)],
            got.at[n : 2 * n, :, pl.ds(c * chunk, chunk)],
            send.at[step + 2, c],
            recv.at[step + 2, c],
            partners[step],
        )
        copies[step + 1, 0, c].start()

    for step in range(bits):
        n = half >> step
        source = incoming if step == 0 else got
        shift = 0 if step == 0 else n
        for c in range(chunks):
            copies[step + 1, 0, c].wait_recv()
            cols = slice(c * chunk, (c + 1) * chunk)
            if step + 1 < bits:
                add_into(acc, source, n // 2, n, shift, cols)
                exchange(step + 1, c)
                add_into(acc, source, 0, n // 2, shift, cols)
            else:
                out_ref[:, cols] = acc[0, :, cols].astype(F32) + source[
                    shift, :, cols
                ].astype(F32)
    for key in copies:
        copies[key].wait_send()


def communicate(kernel, out_shape, scratch, number, *operands):
    whole = pl.BlockSpec(memory_space=VMEM)
    many = isinstance(out_shape, tuple)
    return pl.pallas_call(
        kernel,
        out_shape=out_shape,
        in_specs=[whole] * len(operands),
        out_specs=(whole,) * len(out_shape) if many else whole,
        scratch_shapes=scratch,
        compiler_params=pltpu.CompilerParams(
            collective_id=number, has_side_effects=True, vmem_limit_bytes=50 * 1024 * 1024
        ),
    )(*operands)


def body(
    tokens,
    norm_gain_attn,
    w_query,
    w_key,
    w_value,
    w_forget,
    forget_bias,
    cache_keys,
    cache_values,
    cache_logcum,
    lengths,
    w_out,
    norm_gain_mix,
    norm_gain_ffn,
    expert_gate,
    expert_up,
    expert_down,
    routes,
    route_weights,
):
    row_count = tokens.shape[0]
    model_width = tokens.shape[1]
    query_cols = w_query.shape[1]
    key_cols = w_key.shape[1]
    residual = tokens.astype(jnp.float32)
    normed = rms_scaled(residual, norm_gain_attn).astype(jnp.bfloat16)
    devices = lax.axis_size("ep")
    expert_count = devices // SPAN
    slot_count = max(2, min(row_count, 2 * row_count * TOP // expert_count))
    depth = w_query.shape[0]
    joint_cols = query_cols + 2 * key_cols
    chunk = 256
    dense = (
        slot_count == row_count
        and lax.axis_size("tp") == 2
        and devices & (devices - 1) == 0
        and depth % 128 == 0
        and joint_cols % chunk == 0
        and model_width % (2 * chunk) == 0
    )
    if dense:
        bits = bit_count(devices)
        dma = pltpu.SemaphoreType.DMA
        projected = communicate(
            functools.partial(project_kernel, devices, chunk),
            jax.ShapeDtypeStruct((row_count, joint_cols), BF16),
            [
                VMEM((devices, row_count, depth), BF16),
                VMEM((devices, row_count, joint_cols), BF16),
                VMEM((devices, row_count, joint_cols), BF16),
                dma((devices,)),
                dma((devices,)),
                dma((bits, joint_cols // chunk)),
                dma((bits, joint_cols // chunk)),
            ],
            1,
            normed,
            w_query,
            w_key,
            w_value,
        )
    else:
        joined = jnp.concatenate(
            (
                lax.all_gather(w_query, "ep", axis=0, tiled=True),
                lax.all_gather(w_key, "ep", axis=0, tiled=True),
                lax.all_gather(w_value, "ep", axis=0, tiled=True),
            ),
            axis=1,
        )
        projected = jnp.dot(normed, joined, preferred_element_type=jnp.float32)
    query = projected[:, :query_cols].astype(jnp.bfloat16)
    new_keys = projected[:, query_cols : query_cols + key_cols].astype(jnp.bfloat16)
    new_values = projected[:, query_cols + key_cols :].astype(jnp.bfloat16)
    new_log_gate = jax.nn.log_sigmoid(
        jnp.dot(normed, w_forget, preferred_element_type=jnp.float32) + forget_bias
    )
    local_heads = query_cols // HEAD_DIM
    local_kv = key_cols // HEAD_DIM
    group = HEAD_TOTAL // KV_HEADS
    span_len = cache_keys.shape[2]
    scale = HEAD_DIM ** (-0.5)
    query_heads = query.reshape(row_count, local_kv, group, HEAD_DIM)
    key_heads = cache_keys.reshape(row_count, local_kv, HEAD_DIM, span_len)
    value_heads = cache_values.reshape(row_count, local_kv, HEAD_DIM, span_len)
    scores = jnp.einsum(
        "bkgd,bkdl->bkgl", query_heads, key_heads, preferred_element_type=jnp.float32
    )
    scores = scores.reshape(row_count, local_heads, span_len) * scale
    own_key = new_keys.astype(jnp.float32).reshape(row_count, local_kv, 1, HEAD_DIM)
    own_score = (
        jnp.sum(query_heads.astype(jnp.float32) * own_key, axis=-1).reshape(row_count, local_heads)
        * scale
    )
    places = jnp.arange(span_len, dtype=jnp.int32)
    at_last = (places[None, :] == (lengths - 1)[:, None]).astype(jnp.float32)
    last_cum = jnp.sum(cache_logcum * at_last[:, None, :], axis=2)
    shift = (last_cum + new_log_gate)[:, :, None] - cache_logcum
    valid = (places[None, :] < lengths[:, None])[:, None, :]
    past = jnp.where(valid, scores + shift, MASKED)
    peak = jnp.maximum(jnp.max(past, axis=-1), own_score)
    past_exp = jnp.exp(past - peak[:, :, None])
    own_exp = jnp.exp(own_score - peak)
    total = jnp.sum(past_exp, axis=-1) + own_exp
    past_weight = (
        (past_exp / total[:, :, None])
        .astype(jnp.bfloat16)
        .reshape(row_count, local_kv, group, span_len)
    )
    own_weight = (
        (own_exp / total)
        .astype(jnp.bfloat16)
        .astype(jnp.float32)
        .reshape(row_count, local_kv, group)
    )
    mixed = jnp.einsum(
        "bkgl,bkdl->bkgd", past_weight, value_heads, preferred_element_type=jnp.float32
    )
    own_value = new_values.astype(jnp.float32).reshape(row_count, local_kv, 1, HEAD_DIM)
    mixed = mixed + own_weight[:, :, :, None] * own_value
    heads_out = mixed.astype(jnp.bfloat16).reshape(row_count, query_cols)
    partial_mix = (
        jnp.dot(heads_out, w_out, preferred_element_type=jnp.float32)
        .astype(jnp.bfloat16)
        .astype(jnp.float32)
    )
    if dense:
        chosen = (routes[:, :, None] == jnp.arange(expert_count, dtype=jnp.int32)).astype(F32)
        weights = jnp.sum(chosen * route_weights[:, :, None], axis=1)
        upper = weights.astype(BF16)
        lower = (weights - upper.astype(F32)).astype(BF16)
        lanes = 128
        weights = jnp.concatenate((upper, lower), axis=1)
        weights = jnp.pad(weights, ((0, 0), (0, lanes - weights.shape[1])))
        pieces = model_width // (2 * chunk)
        mixed_res, rows_all, weights_all = communicate(
            functools.partial(dispatch_kernel, devices, pieces),
            (
                jax.ShapeDtypeStruct((row_count, model_width), F32),
                jax.ShapeDtypeStruct((devices, row_count, model_width), BF16),
                jax.ShapeDtypeStruct((devices, row_count, lanes), BF16),
            ),
            [
                VMEM((row_count, model_width), BF16),
                dma((2,)),
                dma((2,)),
                dma((bits, pieces)),
                dma((bits, pieces)),
                dma((bits,)),
                dma((bits,)),
            ],
            2,
            partial_mix.astype(BF16),
            tokens,
            norm_gain_mix.reshape(1, -1),
            norm_gain_ffn.reshape(1, -1),
            weights,
        )
        flat_rows = rows_all.reshape(devices * row_count, model_width)
        gate_part = jnp.dot(flat_rows, expert_gate, preferred_element_type=F32)
        up_part = jnp.dot(flat_rows, expert_up, preferred_element_type=F32)
        hidden = (jax.nn.silu(gate_part) * up_part).astype(BF16)
        expert_part = jnp.dot(hidden, expert_down, preferred_element_type=F32)
        mine = lax.axis_index("ep") // SPAN
        lane = jnp.arange(lanes, dtype=jnp.int32)
        picked = ((lane == mine) | (lane == mine + expert_count)).astype(F32)
        own_weight = jnp.sum(weights_all.astype(F32) * picked, axis=2).reshape(-1, 1)
        share = model_width // 2
        part = (expert_part * own_weight).astype(BF16)
        half = devices // 2
        routed = communicate(
            functools.partial(combine_kernel, devices, chunk),
            jax.ShapeDtypeStruct((row_count, share), F32),
            [
                VMEM((half, row_count, share), BF16),
                VMEM((2, half, row_count, share), BF16),
                VMEM((2, half, row_count, share), BF16),
                VMEM((half, row_count, share), BF16),
                dma((bits + 2, share // chunk)),
                dma((bits + 2, share // chunk)),
            ],
            3,
            part.reshape(devices, row_count, model_width),
        )
        residual_cols = lax.dynamic_slice_in_dim(
            mixed_res, lax.axis_index("tp") * share, share, 1
        )
        layer_out = (residual_cols + routed).astype(BF16)
        return (layer_out, new_keys, new_values, new_log_gate)
    mix = lax.psum(partial_mix.astype(jnp.bfloat16), "tp").astype(jnp.float32)
    mixed_res = residual + rms_scaled(mix, norm_gain_mix)
    ffn_in = rms_scaled(mixed_res, norm_gain_ffn).astype(jnp.bfloat16)
    flat_routes = routes.reshape(-1)
    expert_hits = (
        flat_routes[:, None] == jnp.arange(expert_count, dtype=jnp.int32)[None, :]
    ).astype(jnp.int32)
    earlier = jnp.cumsum(expert_hits, axis=0) - expert_hits
    slot_index = jnp.sum(earlier * expert_hits, axis=1)
    in_slot = (slot_index[:, None] == jnp.arange(slot_count, dtype=jnp.int32)[None, :]).astype(
        jnp.float32
    )
    placing = expert_hits.astype(jnp.float32)[:, :, None] * in_slot[:, None, :]
    placing = placing.reshape(row_count, TOP, expert_count * slot_count)
    selector = jnp.sum(placing, axis=1).astype(jnp.bfloat16)
    weighing = jnp.sum(placing * route_weights[:, :, None], axis=1)
    packed = jnp.einsum("ra,rd->ad", selector, ffn_in, preferred_element_type=jnp.float32).astype(
        jnp.bfloat16
    )
    outgoing = jnp.broadcast_to(
        packed.reshape(expert_count, 1, slot_count, model_width),
        (expert_count, SPAN, slot_count, model_width),
    )
    outgoing = outgoing.reshape(expert_count * SPAN, slot_count, model_width)
    arrived = lax.all_to_all(outgoing, "ep", split_axis=0, concat_axis=0, tiled=True)
    sources, slots, width = arrived.shape
    flat_rows = arrived.reshape(sources * slots, width)
    gate_part = jnp.dot(flat_rows, expert_gate, preferred_element_type=jnp.float32)
    up_part = jnp.dot(flat_rows, expert_up, preferred_element_type=jnp.float32)
    hidden = (jax.nn.silu(gate_part) * up_part).astype(jnp.bfloat16)
    expert_part = jnp.dot(hidden, expert_down, preferred_element_type=jnp.float32)
    col_share = lax.psum_scatter(
        expert_part.astype(jnp.bfloat16), "tp", scatter_dimension=1, tiled=True
    ).astype(jnp.float32)
    returned = lax.all_to_all(
        col_share.reshape(sources, slots, -1).astype(jnp.bfloat16),
        "ep",
        split_axis=0,
        concat_axis=0,
        tiled=True,
    ).astype(jnp.float32)
    col_width = returned.shape[2]
    per_expert = jnp.sum(returned.reshape(expert_count, SPAN, slot_count, col_width), axis=1)
    per_expert = per_expert.reshape(expert_count * slot_count, col_width)
    routed = jnp.dot(
        weighing, per_expert, precision=lax.Precision.HIGHEST, preferred_element_type=jnp.float32
    )
    col_start = lax.axis_index("tp") * col_width
    residual_cols = lax.dynamic_slice_in_dim(mixed_res, col_start, col_width, 1)
    layer_out = (residual_cols + routed).astype(jnp.bfloat16)
    return (layer_out, new_keys, new_values, new_log_gate)


def solution(mesh):
    placed = (
        P("ep", None),
        P(),
        P("ep", "tp"),
        P("ep", "tp"),
        P("ep", "tp"),
        P(None, "tp"),
        P("tp"),
        P("ep", "tp", None),
        P("ep", "tp", None),
        P("ep", "tp", None),
        P("ep"),
        P("tp", None),
        P(),
        P(),
        P(None, ("ep", "tp")),
        P(None, ("ep", "tp")),
        P(("ep", "tp"), None),
        P("ep", None),
        P("ep", None),
    )
    return jax.shard_map(
        body,
        mesh=mesh,
        in_specs=placed,
        out_specs=(P("ep", "tp"), P("ep", "tp"), P("ep", "tp"), P("ep", "tp")),
        check_vma=False,
    )
```

profile of v0, /device:TPU:0, one launch (start us, length us, event | category | flops | bytes accessed | tf_op | source)
XLA Modules:
  0.0 120.6 jit_solution(3947135648831710765)
XLA Ops:
  0.7 0.8 broadcast_add_fusion
  1.5 1.0 fusion.8
  2.5 0.7 select_reduce_fusion
  3.3 0.1 copy.62
  3.4 0.7 iota_compare_fusion.1
  4.1 1.0 fusion.10.x_ref
  5.2 0.9 copy-done.3
  6.1 0.8 copy-done.4
  6.9 0.8 copy-done.5
  7.6 26.9 %shard_map.210 = bf16[32,1280]{1,0:T(8,128)(2,1)S(1)} custom-call(bf16[32,2048]{1,0:T(8,128)(2,1)S(1)} %fusion.10.x_ref, bf16[128,1024]{1,0:T(8,128)(2,1)S(1)} %copy-done.3, bf16[128,128]{1,0:T(8,128)(2,1)S(1)} %copy-done.4, bf16[128,128]{1,0:T(8,128)(2,1)S(1)} %copy-done.5), custom_call_target="tpu_custom_call" | custom-call | tf_op jit(solution)/shard_map/pallas_call | solution.py:318
  34.6 0.1 reshape.149
  34.7 0.1 reshape.148
  34.8 0.1 reshape.139
  34.9 0.2 multiply_reduce_fusion.2
  35.2 0.1 fusion.11
  35.3 1.9 %multiply_reduce_fusion = f32[32,16]{1,0:T(8,128)S(1)} fusion(f32[32,16,1024]{2,1,0:T(8,128)} %param.28, f32[32,1024]{1,0:T(8,128)S(1)} %fusion.11), kind=kLoop, calls=%fused_computation.6 | loop fusion | flops 1048064 | bytes 2230272 | tf_op jit(solution)/shard_map/reduce_sum | solution.py:427
  37.3 0.8 fusion.18
  38.2 6.6 %fusion.19 = (f32[32,16]{1,0:T(8,128)S(1)}, f32[32,16,1024]{2,1,0:T(8,128)}) fusion(f32[32,16,1024]{2,1,0:T(8,128)} %param.28, f32[32,16]{1,0:T(8,128)S(1)} %copy.55, bf16[32,2,8,64]{3,2,1,0:T(8,128)(2,1)S(1)} %reshape.139, bf16[32,2,64,1024]{3,2,1,0:T(8,128)(2,1)} %bitcast.46, pred[32,1024]{1,0:T(8,128)(4,1)S(1)} %iota_compare_fusion.1), kind=kOutput, calls=%fused_computation.47 | convolution fusion | flops 69729792 | bytes 12685312 | tf_op jit(solution)/shard_map/bkgd,bkdl->bkgl/dot_general | solution.py:416
  44.8 2.0 %fusion.1 = f32[32,16]{1,0:T(8,128)S(1)} fusion(f32[32,16,1024]{2,1,0:T(8,128)} %get-tuple-element.17, f32[32,16]{1,0:T(8,128)S(1)} %max.28), kind=kLoop, calls=%fused_computation.7 | loop fusion | flops 1048064 | bytes 2101248 | tf_op jit(solution)/shard_map/reduce_sum | solution.py:434
  47.0 0.1 copy.61
  47.1 6.4 %fusion.3 = bf16[32,2,8,64]{3,2,1,0:T(8,128)(2,1)S(1)} fusion(bf16[32,2,64,1024]{3,2,1,0:T(8,128)(2,1)} %bitcast.47, f32[32,16,1024]{2,1,0:T(8,128)} %get-tuple-element.17, f32[32,16]{1,0:T(8,128)S(1)} %exponential_add_fusion, f32[32,16]{1,0:T(8,128)S(1)} %max.28, f32[32,2,64]{2,1,0:T(2,128)S(1)} %reshape.149, f32[32,2,8]{2,1,0:T(2,128)S(1)} %copy.61), kind=kOutput, calls=%fused_computation.11 | convolution fusion | flops 68780032 | bytes 10573824 | tf_op jit(solution)/shard_map/bkgl,bkdl->bkgd/dot_general | solution.py:446
  53.4 0.2 reshape.143
  53.6 3.1 %convolution_convert_fusion.part_ref = bf16[32,2048]{1,0:T(8,128)(2,1)S(1)} fusion(bf16[32,1024]{1,0:T(8,128)(2,1)S(1)} %reshape.143, bf16[1024,2048]{1,0:T(8,128)(2,1)} %param.30), kind=kOutput, calls=%fused_computation.1 | convolution fusion | flops 134283264 | bytes 4390912 | tf_op jit(solution)/shard_map/dot_general | solution.py:453
  56.7 23.3 %shard_map.211 = (f32[32,2048]{1,0:T(8,128)S(1)}, bf16[16,32,2048]{2,1,0:T(8,128)(2,1)S(1)}, bf16[16,32,128]{2,1,0:T(8,128)(2,1)S(1)}) custom-call(bf16[32,2048]{1,0:T(8,128)(2,1)S(1)} %convolution_convert_fusion.part_ref, bf16[32,2048]{1,0:T(8,128)(2,1)S(1)} %copy-done.2, f32[1,2048]{1,0:T(1,128)S(1)} %bitcast.42, f32[1,2048]{1,0:T(1,128)S(1)} %bitcast.43, ...), custom_call_target="tpu_custom_call" | custom-call | tf_op jit(solution)/shard_map/pallas_call | solution.py:318
  80.1 1.3 %copy-done.8 = bf16[16,32,2048]{2,1,0:T(8,128)(2,1)} copy-done((bf16[16,32,2048]{2,1,0:T(8,128)(2,1)}, bf16[16,32,2048]{2,1,0:T(8,128)(2,1)S(1)}, u32[]{:S(2)}) %copy-start.8) | copy-done | bytes 2097176
  81.4 0.1 multiply_reduce_fusion.1
  81.5 0.1 mul.152
  81.6 3.5 %fusion.20 = f32[512,512]{1,0:T(8,128)S(1)} fusion(bf16[512,2048]{1,0:T(8,128)(2,1)} %bitcast.44, bf16[2048,512]{1,0:T(8,128)(2,1)} %param.33), kind=kOutput, calls=%fused_computation.48 | convolution fusion | flops 1073741824 | bytes 5242880 | tf_op jit(solution)/shard_map/dot_general | solution.py:490
  85.1 6.0 %multiply_convert_fusion = bf16[512,2048]{1,0:T(8,128)(2,1)} fusion(bf16[512,2048]{1,0:T(8,128)(2,1)S(1)} %copy-done, f32[512]{0:T(512)S(1)} %mul.152, bf16[512,2048]{1,0:T(8,128)(2,1)} %bitcast.45, bf16[2048,512]{1,0:T(8,128)(2,1)} %param.34, f32[512,512]{1,0:T(8,128)S(1)} %fusion.20), kind=kOutput, calls=%fused_computation | convolution fusion | flops 2151153664 | bytes 9439232 | tf_op jit(solution)/shard_map/dot_general | solution.py:493
  91.1 1.6 %copy-done.1 = bf16[512,2048]{1,0:T(8,128)(2,1)S(1)} copy-done((bf16[512,2048]{1,0:T(8,128)(2,1)S(1)}, bf16[512,2048]{1,0:T(8,128)(2,1)}, u32[]{:S(2)}) %copy-start.1) | copy-done | bytes 2097176
  92.7 27.2 %shard_map.212 = f32[32,1024]{1,0:T(8,128)S(1)} custom-call(bf16[16,32,2048]{2,1,0:T(8,128)(2,1)S(1)} %bitcast.41), custom_call_target="tpu_custom_call" | custom-call | tf_op jit(solution)/shard_map/pallas_call | solution.py:318
  119.9 0.7 add_convert_fusion
  (38 shorter events, 0.6 us)
Async XLA Ops:
  0.6 84.5 %copy-start = (bf16[512,2048]{1,0:T(8,128)(2,1)S(1)}, bf16[512,2048]{1,0:T(8,128)(2,1)}, u32[]{:S(2)}) copy-start(bf16[512,2048]{1,0:T(8,128)(2,1)} %param.35) | copy-start | bytes 6291460
  0.7 36.7 %copy-start.9 = (bf16[2048,16]{0,1:T(8,128)(2,1)S(1)}, bf16[2048,16]{0,1:T(8,128)(2,1)}, u32[]{:S(2)}) copy-start(bf16[2048,16]{0,1:T(8,128)(2,1)} %param.24) | copy-start | bytes 196612
  0.7 36.7 %copy-start.12 = (f32[16]{0:T(128)S(1)}, f32[16]{0:T(128)}, u32[]{:S(2)}) copy-start(f32[16]{0:T(128)} %param.25) | copy-start | bytes 196
  5.1 1.0 copy-start.3
  6.1 0.8 copy-start.4
  6.9 0.8 copy-start.5
  34.5 10.2 %copy-start.10 = (bf16[32,128]{1,0:T(8,128)(2,1)}, bf16[32,128]{1,0:T(8,128)(2,1)S(1)}, u32[]{:S(2)}) copy-start(bf16[32,128]{1,0:T(8,128)(2,1)S(1)} %get-tuple-element.12) | copy-start | bytes 24580
  34.6 10.2 %copy-start.11 = (bf16[32,128]{1,0:T(8,128)(2,1)}, bf16[32,128]{1,0:T(8,128)(2,1)S(1)}, u32[]{:S(2)}) copy-start(bf16[32,128]{1,0:T(8,128)(2,1)S(1)} %get-tuple-element.13) | copy-start | bytes 24580
  53.6 3.1 %copy-start.2 = (bf16[32,2048]{1,0:T(8,128)(2,1)S(1)}, bf16[32,2048]{1,0:T(8,128)(2,1)}, u32[]{:S(2)}) copy-start(bf16[32,2048]{1,0:T(8,128)(2,1)} %tok_ref.1) | copy-start | bytes 393220
  53.6 3.1 %copy-start.6 = (f32[2048]{0:T(1024)S(1)}, f32[2048]{0:T(1024)}, u32[]{:S(2)}) copy-start(f32[2048]{0:T(1024)} %param.31) | copy-start | bytes 24580
  53.6 3.1 %copy-start.7 = (f32[2048]{0:T(1024)S(1)}, f32[2048]{0:T(1024)}, u32[]{:S(2)}) copy-start(f32[2048]{0:T(1024)} %param.32) | copy-start | bytes 24580
  80.0 1.4 %copy-start.8 = (bf16[16,32,2048]{2,1,0:T(8,128)(2,1)}, bf16[16,32,2048]{2,1,0:T(8,128)(2,1)S(1)}, u32[]{:S(2)}) copy-start(bf16[16,32,2048]{2,1,0:T(8,128)(2,1)S(1)} %get-tuple-element.8) | copy-start | bytes 6291460
  91.1 1.6 %copy-start.1 = (bf16[512,2048]{1,0:T(8,128)(2,1)S(1)}, bf16[512,2048]{1,0:T(8,128)(2,1)}, u32[]{:S(2)}) copy-start(bf16[512,2048]{1,0:T(8,128)(2,1)} %multiply_convert_fusion) | copy-start | bytes 6291460
where the time goes:
time: 121 us
  Pallas kernels  77.4 us (64%)
  matrix products  26.3 us (22%)
  other arithmetic  9.38 us (8%)
  local copies, waits for them, and re-layouts  6.63 us (5%)
    pallas_call x3, Pallas kernels, communicate(): pl.pallas_call(kernel, out_shape=out_shape, in_specs=[whole] * len(operan...  77.4 us
    dot_general x1, matrix products, body(): jnp.einsum('bkgd,bkdl->bkgl', query_heads, key_heads, preferred_element_t...  6.56 us
    dot_general x1, matrix products, body(): jnp.einsum('bkgl,bkdl->bkgd', past_weight, value_heads, preferred_element...  6.36 us
    dot_general x1, matrix products, body(): expert_part = jnp.dot(hidden, expert_down, preferred_element_type=F32)  6 us
    unnamed x26, local copies, waits for them, and re-layouts  5.45 us
    dot_general x1, matrix products, body(): gate_part = jnp.dot(flat_rows, expert_gate, preferred_element_type=F32)  3.46 us
    dot_general x1, matrix products, body(): jnp.dot(heads_out, w_out, preferred_element_type=jnp.float32)  3.07 us

commit v1 on v0

--- a/solution.py
+++ b/solution.py
@@ -70,92 +70,327 @@
     ).astype(BF16)
 
 
-def project_kernel(
-    devices, chunk, x_ref, wq_ref, wk_ref, wv_ref, out_ref, xs, acc, got, xsend, xrecv, send, recv
+def copy_of(src, dst, sem):
+    return pltpu.make_async_copy(src_ref=src, dst_ref=dst, sem=sem)
+
+
+def normalized(field):
+    return field * lax.rsqrt(jnp.mean(field * field, axis=-1, keepdims=True) + EPSILON)
+
+
+def front_kernel(
+    zs,
+    chunk,
+    tok_hbm,
+    gain_hbm,
+    wq_hbm,
+    wk_hbm,
+    wv_hbm,
+    wf_hbm,
+    bias_hbm,
+    kc_hbm,
+    vc_hbm,
+    cum_hbm,
+    len_hbm,
+    wo_hbm,
+    gmix_hbm,
+    gffn_hbm,
+    nk_ref,
+    nv_ref,
+    gate_ref,
+    res_ref,
+    ffn_ref,
+    tok,
+    gattn,
+    gmix,
+    gffn,
+    weights,
+    wf,
+    bias,
+    kc,
+    vc,
+    cum,
+    lens,
+    wo,
+    normed,
+    xs,
+    own,
+    acc,
+    got,
+    qs,
+    kn,
+    vn,
+    scores,
+    probs,
+    own_exp,
+    inverse,
+    outs,
+    heads,
+    part,
+    theirs,
+    local,
+    xsend,
+    xrecv,
+    csend,
+    crecv,
+    fsend,
+    frecv,
+    tsend,
+    trecv,
+    zsend,
+    zrecv,
+    ysend,
+    yrecv,
 ):
-    bits = bit_count(devices)
     me, tp = lax.axis_index("ep"), lax.axis_index("tp")
-    rows, depth = xs.shape[1], xs.shape[2]
-    total = acc.shape[2]
-    greet([(flipped(me, m, bits), tp) for m in range(1, devices)])
-    moves = {}
-    for s in range(devices - 1, 0, -1):
-        other = flipped(me, reversed_bits(s, bits), bits)
-        cols = pl.ds(pl.multiple_of(other * depth, depth), depth)
-        moves[s] = remote(x_ref.at[:, cols], xs.at[s], xsend.at[s], xrecv.at[s], (other, tp))
-        moves[s].start()
-    own = pltpu.make_async_copy(
-        x_ref.at[:, pl.ds(pl.multiple_of(me * depth, depth), depth)], xs.at[0], xrecv.at[0]
-    )
-    own.start()
-    own.wait()
-    half = devices // 2
-    copies = {}
-
-    def exchange(step, c):
-        n = half >> step
-        cols = pl.ds(c * chunk, chunk)
-        other = flipped(me, 1 << step, bits)
-        copies[step, c] = remote(
-            acc.at[n : 2 * n, :, cols],
-            got.at[n : 2 * n, :, cols],
-            send.at[step, c],
-            recv.at[step, c],
-            (other, tp),
+    place = me % SPAN
+    z = me // SPAN
+    core_peer = (me + 1 - 2 * (me % 2), tp)
+    x_peer = (me + 2 - 4 * ((me // 2) % 2), tp)
+    y_peer = (me, 1 - tp)
+
+    def z_peer(d):
+        return (((z + d + zs) % zs) * SPAN + place, tp)
+
+    rows, width = tok.shape
+    depth = wq_hbm.shape[0]
+    query_cols = wq_hbm.shape[1]
+    key_cols = wk_hbm.shape[1]
+    slab = SPAN * depth
+    total = weights.shape[1]
+    chunks = total // chunk
+    heads_here = query_cols // HEAD_DIM
+    mine = pl.ds(pl.multiple_of(place * depth, depth), depth)
+    x_place = place + 2 - 4 * ((me // 2) % 2)
+    xs_rows = pl.ds(pl.multiple_of(x_place * depth, depth), depth)
+
+    first = [
+        copy_of(tok_hbm, tok, local.at[0]),
+        copy_of(gain_hbm, gattn, local.at[1]),
+        copy_of(wq_hbm, weights.at[mine, 0:query_cols], local.at[2]),
+        copy_of(wk_hbm, weights.at[mine, query_cols : query_cols + key_cols], local.at[3]),
+        copy_of(wv_hbm, weights.at[mine, query_cols + key_cols : total], local.at[4]),
+        copy_of(wf_hbm, wf, local.at[5]),
+        copy_of(bias_hbm, bias, local.at[6]),
+        copy_of(len_hbm, lens, local.at[7]),
+        copy_of(gmix_hbm, gmix, local.at[8]),
+        copy_of(gffn_hbm, gffn, local.at[9]),
+    ]
+    later = [
+        copy_of(kc_hbm, kc, local.at[10]),
+        copy_of(vc_hbm, vc, local.at[11]),
+        copy_of(cum_hbm, cum, local.at[12]),
+        copy_of(wo_hbm, wo, local.at[13]),
+    ]
+    for move in first:
+        move.start()
+    barrier = pltpu.get_barrier_semaphore()
+    partners = [core_peer, x_peer, y_peer] + [z_peer(d) for d in range(1, zs)]
+    for partner in partners:
+        pl.semaphore_signal(barrier, inc=1, device_id=partner, device_id_type=MESH)
+    first[0].wait()
+    first[1].wait()
+    normed[...] = (normalized(tok[...].astype(F32)) * gattn[...]).astype(BF16)
+    xs[0:rows, :] = normed[:, pl.ds(pl.multiple_of(z * slab, slab), slab)]
+    for move in first[2:5]:
+        move.wait()
+    pl.semaphore_wait(barrier, len(partners))
+
+    order = [chunks - 1] + list(range(chunks - 1))
+    across, direct, forward, slabs, sums = {}, {}, {}, {}, {}
+    for k in order:
+        cols = pl.ds(k * chunk, chunk)
+        view = weights.at[mine, cols]
+        across[k] = remote(view, view, xsend.at[k], xrecv.at[k], x_peer)
+        across[k].start()
+        if k == order[0]:
+            for d in range(1, zs):
+                peer = z_peer(d)
+                there = pl.ds(pl.multiple_of((peer[0] // SPAN) * slab, slab), slab)
+                slabs[d] = remote(
+                    normed.at[:, there],
+                    xs.at[d * rows : (d + 1) * rows],
+                    tsend.at[d],
+                    trecv.at[d],
+                    peer,
+                )
+                slabs[d].start()
+    view = weights.at[mine]
+    direct = remote(view, view, csend.at[0], crecv.at[0], core_peer)
+    direct.start()
+    for move in later:
+        move.start()
+
+    for move in first[5:7]:
+        move.wait()
+    logits = lax.dot_general(
+        wf[...], normed[...], (((1,), (1,)), ((), ())), preferred_element_type=F32
+    )
+    row_of = lax.broadcasted_iota(jnp.int32, logits.shape, 0)
+    for h in range(heads_here):
+        logits = logits + jnp.where(row_of == h, bias[h], 0.0)
+    gate_ref[...] = jnp.minimum(logits, 0.0) - jnp.log1p(jnp.exp(-jnp.abs(logits)))
+
+    for d in range(1, zs):
+        slabs[d].wait_recv()
+    direct.wait_recv()
+    for k in order:
+        cols = pl.ds(k * chunk, chunk)
+        across[k].wait_recv()
+        view = weights.at[xs_rows, cols]
+        forward[k] = remote(view, view, fsend.at[k], frecv.at[k], core_peer)
+        forward[k].start()
+        forward[k].wait_recv()
+        product = jnp.dot(xs[...], weights[:, cols], preferred_element_type=F32)
+        own[k] = product[0:rows]
+        acc[k] = product[rows:].astype(BF16)
+        for d in range(1, zs):
+            sums[k, d] = remote(
+                acc.at[k, (d - 1) * rows : d * rows],
+                got.at[k, (d - 1) * rows : d * rows],
+                zsend.at[k, d],
+                zrecv.at[k, d],
+                z_peer(-d),
+            )
+            sums[k, d].start()
+
+    lane = lax.broadcasted_iota(jnp.int32, (rows, 2 * HEAD_DIM), 1)
+    low = lane < HEAD_DIM
+    for k in order:
+        value = own[k]
+        for d in range(1, zs):
+            sums[k, d].wait_recv()
+            value = value + got[k, (d - 1) * rows : d * rows, :].astype(F32)
+        value = value.astype(BF16)
+        if k == order[0]:
+            nk_ref[...] = value[:, 0:key_cols]
+            nv_ref[...] = value[:, key_cols:]
+            kn[...] = value[:, 0:key_cols].astype(F32)
+            vn[...] = value[:, key_cols:].astype(F32)
+            continue
+        value = value.astype(F32) * (HEAD_DIM**-0.5)
+        for j in range(chunk // (2 * HEAD_DIM)):
+            block = value[:, j * 2 * HEAD_DIM : (j + 1) * 2 * HEAD_DIM]
+            rolled = pltpu.roll(block, HEAD_DIM, 1)
+            head = (k * chunk) // HEAD_DIM + 2 * j
+            if head < heads_here // 2:
+                pair = (jnp.where(low, block, 0.0), jnp.where(low, rolled, 0.0))
+            else:
+                pair = (jnp.where(low, 0.0, rolled), jnp.where(low, 0.0, block))
+            qs[pl.ds(head, rows, stride=heads_here), :] = pair[0]
+            qs[pl.ds(head + 1, rows, stride=heads_here), :] = pair[1]
+
+    for move in later:
+        move.wait()
+    first[7].wait()
+    unroll = 4
+    groups = rows // unroll
+    span_len = cum.shape[2]
+    places = lax.broadcasted_iota(jnp.int32, (heads_here, span_len), 1)
+    lane_b = lax.broadcasted_iota(jnp.int32, gate_ref.shape, 1)
+
+    def strip(b):
+        return pl.ds(pl.multiple_of(b * heads_here, heads_here), heads_here)
+
+    def score(g):
+        for u in range(unroll):
+            b = g * unroll + u
+            scores[strip(b), :] = jnp.dot(
+                qs[strip(b), :].astype(BF16), kc[b], preferred_element_type=F32
+            )
+
+    def soften(g):
+        for u in range(unroll):
+            b = g * unroll + u
+            length = lens[b]
+            logcum = cum[b]
+            gate = jnp.sum(jnp.where(lane_b == b, gate_ref[...], 0.0), axis=1, keepdims=True)
+            last = jnp.sum(jnp.where(places == length - 1, logcum, 0.0), axis=1, keepdims=True)
+            mine_score = jnp.sum(qs[strip(b), :] * kn[pl.ds(b, 1), :], axis=1, keepdims=True)
+            past = scores[strip(b), :] + ((last + gate) - logcum)
+            past = jnp.where(places < length, past, MASKED)
+            peak = jnp.maximum(jnp.max(past, axis=1, keepdims=True), mine_score)
+            raised = jnp.exp(past - peak)
+            mine_exp = jnp.exp(mine_score - peak)
+            probs[strip(b), :] = raised.astype(BF16)
+            sum_all = jnp.sum(raised, axis=1, keepdims=True) + mine_exp
+            own_exp[strip(b), :] = jnp.broadcast_to(mine_exp, (heads_here, key_cols))
+            inverse[strip(b), :] = jnp.broadcast_to(1.0 / sum_all, (heads_here, key_cols))
+
+    def weigh(g):
+        for u in range(unroll):
+            b = g * unroll + u
+            mixed = lax.dot_general(
+                probs[strip(b), :],
+                vc[b],
+                (((1,), (1,)), ((), ())),
+                preferred_element_type=F32,
+            )
+            mixed = mixed + own_exp[strip(b), :] * vn[pl.ds(b, 1), :]
+            outs[strip(b), :] = mixed * inverse[strip(b), :]
+
+    def turn(g, carry):
+        weigh(g - 2)
+        soften(g - 1)
+        score(g)
+        return carry
+
+    score(0)
+    soften(0)
+    score(1)
+    lax.fori_loop(2, groups, turn, 0)
+    weigh(groups - 2)
+    soften(groups - 1)
+    weigh(groups - 1)
+
+    for m in range(heads_here // 2):
+        a = outs[pl.ds(2 * m, rows, stride=heads_here), :]
+        b = outs[pl.ds(2 * m + 1, rows, stride=heads_here), :]
+        if 2 * m < heads_here // 2:
+            b = pltpu.roll(b, HEAD_DIM, 1)
+        else:
+            a = pltpu.roll(a, HEAD_DIM, 1)
+        heads[:, m * 2 * HEAD_DIM : (m + 1) * 2 * HEAD_DIM] = jnp.where(low, a, b).astype(BF16)
+
+    piece = 2 * chunk
+    swaps = {}
+    for n in range(width // piece):
+        cols = pl.ds(n * piece, piece)
+        part[:, cols] = jnp.dot(
+            heads[...], wo[:, cols], preferred_element_type=F32
+        ).astype(BF16)
+        swaps[n] = remote(
+            part.at[:, cols], theirs.at[:, cols], ysend.at[n], yrecv.at[n], y_peer
         )
-        copies[step, c].start()
-
-    def multiply(low, high):
-        left = xs[low:high].reshape((high - low) * rows, depth)
-        start = 0
-        for w_ref in (wq_ref, wk_ref, wv_ref):
-            width = w_ref.shape[1]
-            part = jnp.dot(left, w_ref[...], preferred_element_type=F32)
-            acc[low:high, :, start : start + width] = part.astype(BF16).reshape(
-                high - low, rows, width
-            )
-            start += width
-
-    chunks = total // chunk
-    for s in range(devices - 1, half - 1, -1):
-        moves[s].wait_recv()
-    multiply(half, devices)
-    for c in range(chunks):
-        exchange(0, c)
-    for s in range(half - 1, 0, -1):
-        moves[s].wait_recv()
-    multiply(0, half)
-    for step in range(bits):
-        n = half >> step
-        for c in range(chunks):
-            copies[step, c].wait_recv()
-            cols = slice(c * chunk, (c + 1) * chunk)
-            if step + 1 < bits:
-                add_into(acc, got, n // 2, n, n, cols)
-                exchange(step + 1, c)
-                add_into(acc, got, 0, n // 2, n, cols)
-            else:
-                out_ref[:, cols] = (
-                    acc[0, :, cols].astype(F32) + got[1, :, cols].astype(F32)
-                ).astype(BF16)
-    for s in moves:
-        moves[s].wait_send()
-    for key in copies:
-        copies[key].wait_send()
+        swaps[n].start()
+    for move in first[8:10]:
+        move.wait()
+    for n in swaps:
+        swaps[n].wait_recv()
+    mix = part[...].astype(F32) + theirs[...].astype(F32)
+    mixed_res = tok[...].astype(F32) + normalized(mix) * gmix[...]
+    res_ref[...] = mixed_res
+    ffn_ref[...] = (normalized(mixed_res) * gffn[...]).astype(BF16)
+
+    direct.wait_send()
+    for k in order:
+        across[k].wait_send()
+        forward[k].wait_send()
+    for d in slabs:
+        slabs[d].wait_send()
+    for key in sums:
+        sums[key].wait_send()
+    for n in swaps:
+        swaps[n].wait_send()
 
 
 def dispatch_kernel(
     devices,
     chunks,
-    part_ref,
-    tok_ref,
-    gmix_ref,
-    gffn_ref,
+    rows_ref,
     wts_ref,
-    res_ref,
     all_ref,
     wall_ref,
-    theirs,
     tsend,
     trecv,
     send,
@@ -168,14 +403,8 @@
     other_tp = (me, 1 - tp)
     partners = [(flipped(me, 1 << b, bits), tp) for b in range(bits)]
     greet(partners + [other_tp])
-    swap = remote(part_ref, theirs, tsend.at[0], trecv.at[0], other_tp)
-    swap.start()
     wall_ref[0] = wts_ref[...]
-    swap.wait_recv()
-    mix = part_ref[...].astype(F32) + theirs[...].astype(F32)
-    mixed_res = tok_ref[...].astype(F32) + rms_scaled(mix, gmix_ref[...])
-    res_ref[...] = mixed_res
-    all_ref[0] = rms_scaled(mixed_res, gffn_ref[...]).astype(BF16)
+    all_ref[0] = rows_ref[...]
     width = all_ref.shape[2] // chunks
     copies = {}
     shared = chunks - 2
@@ -228,7 +457,6 @@
     exchange(bits - 1, chunks - 1, theirs_cols)
     for c in order + [chunks - 1]:
         copies[bits - 1, c].wait_recv()
-    swap.wait_send()
     across.wait_send()
     for key in copies:
         copies[key].wait_send()
@@ -312,13 +540,13 @@
         copies[key].wait_send()
 
 
-def communicate(kernel, out_shape, scratch, number, *operands):
+def communicate(kernel, out_shape, scratch, number, *operands, places=VMEM):
     whole = pl.BlockSpec(memory_space=VMEM)
     many = isinstance(out_shape, tuple)
     return pl.pallas_call(
         kernel,
         out_shape=out_shape,
-        in_specs=[whole] * len(operands),
+        in_specs=[pl.BlockSpec(memory_space=places)] * len(operands),
         out_specs=(whole,) * len(out_shape) if many else whole,
         scratch_shapes=scratch,
         compiler_params=pltpu.CompilerParams(
@@ -366,95 +594,91 @@
         and devices & (devices - 1) == 0
         and depth % 128 == 0
         and joint_cols % chunk == 0
+        and devices % SPAN == 0
+        and key_cols == 2 * HEAD_DIM
+        and 2 * key_cols == chunk
+        and row_count % 8 == 0
         and model_width % (2 * chunk) == 0
     )
     if dense:
         bits = bit_count(devices)
         dma = pltpu.SemaphoreType.DMA
-        projected = communicate(
-            functools.partial(project_kernel, devices, chunk),
-            jax.ShapeDtypeStruct((row_count, joint_cols), BF16),
+        zs = devices // SPAN
+        chunks = joint_cols // chunk
+        heads_here = query_cols // HEAD_DIM
+        strips = row_count * heads_here
+        smem = pltpu.SMEM
+        pieces = model_width // (2 * chunk)
+        new_keys, new_values, gate_rows, mixed_res, ffn_in = communicate(
+            functools.partial(front_kernel, zs, chunk),
+            (
+                jax.ShapeDtypeStruct((row_count, key_cols), BF16),
+                jax.ShapeDtypeStruct((row_count, key_cols), BF16),
+                jax.ShapeDtypeStruct((heads_here, row_count), F32),
+                jax.ShapeDtypeStruct((row_count, model_width), F32),
+                jax.ShapeDtypeStruct((row_count, model_width), BF16),
+            ),
             [
-                VMEM((devices, row_count, depth), BF16),
-                VMEM((devices, row_count, joint_cols), BF16),
-                VMEM((devices, row_count, joint_cols), BF16),
-                dma((devices,)),
-                dma((devices,)),
-                dma((bits, joint_cols // chunk)),
-                dma((bits, joint_cols // chunk)),
+                VMEM((row_count, model_width), BF16),
+                VMEM((1, model_width), F32),
+                VMEM((1, model_width), F32),
+                VMEM((1, model_width), F32),
+                VMEM((SPAN * depth, joint_cols), BF16),
+                VMEM((heads_here, model_width), BF16),
+                smem((heads_here,), F32),
+                VMEM(cache_keys.shape, BF16),
+                VMEM(cache_values.shape, BF16),
+                VMEM(cache_logcum.shape, F32),
+                smem((row_count,), jnp.int32),
+                VMEM(w_out.shape, BF16),
+                VMEM((row_count, model_width), BF16),
+                VMEM((zs * row_count, SPAN * depth), BF16),
+                VMEM((chunks, row_count, chunk), F32),
+                VMEM((chunks, (zs - 1) * row_count, chunk), BF16),
+                VMEM((chunks, (zs - 1) * row_count, chunk), BF16),
+                VMEM((strips, key_cols), F32),
+                VMEM((row_count, key_cols), F32),
+                VMEM((row_count, key_cols), F32),
+                VMEM((strips, cache_keys.shape[2]), F32),
+                VMEM((strips, cache_keys.shape[2]), BF16),
+                VMEM((strips, key_cols), F32),
+                VMEM((strips, key_cols), F32),
+                VMEM((strips, key_cols), F32),
+                VMEM((row_count, query_cols), BF16),
+                VMEM((row_count, model_width), BF16),
+                VMEM((row_count, model_width), BF16),
+                dma((14,)),
+                dma((chunks,)),
+                dma((chunks,)),
+                dma((1,)),
+                dma((1,)),
+                dma((chunks,)),
+                dma((chunks,)),
+                dma((zs,)),
+                dma((zs,)),
+                dma((chunks, zs)),
+                dma((chunks, zs)),
+                dma((pieces,)),
+                dma((pieces,)),
             ],
             1,
-            normed,
+            tokens,
+            norm_gain_attn.reshape(1, -1),
             w_query,
             w_key,
             w_value,
+            w_forget.T,
+            forget_bias,
+            cache_keys,
+            cache_values,
+            cache_logcum,
+            lengths,
+            w_out,
+            norm_gain_mix.reshape(1, -1),
+            norm_gain_ffn.reshape(1, -1),
+            places=pl.ANY,
         )
-    else:
-        joined = jnp.concatenate(
-            (
-                lax.all_gather(w_query, "ep", axis=0, tiled=True),
-                lax.all_gather(w_key, "ep", axis=0, tiled=True),
-                lax.all_gather(w_value, "ep", axis=0, tiled=True),
-            ),
-            axis=1,
-        )
-        projected = jnp.dot(normed, joined, preferred_element_type=jnp.float32)
-    query = projected[:, :query_cols].astype(jnp.bfloat16)
-    new_keys = projected[:, query_cols : query_cols + key_cols].astype(jnp.bfloat16)
-    new_values = projected[:, query_cols + key_cols :].astype(jnp.bfloat16)
-    new_log_gate = jax.nn.log_sigmoid(
-        jnp.dot(normed, w_forget, preferred_element_type=jnp.float32) + forget_bias
-    )
-    local_heads = query_cols // HEAD_DIM
-    local_kv = key_cols // HEAD_DIM
-    group = HEAD_TOTAL // KV_HEADS
-    span_len = cache_keys.shape[2]
-    scale = HEAD_DIM ** (-0.5)
-    query_heads = query.reshape(row_count, local_kv, group, HEAD_DIM)
-    key_heads = cache_keys.reshape(row_count, local_kv, HEAD_DIM, span_len)
-    value_heads = cache_values.reshape(row_count, local_kv, HEAD_DIM, span_len)
-    scores = jnp.einsum(
-        "bkgd,bkdl->bkgl", query_heads, key_heads, preferred_element_type=jnp.float32
-    )
-    scores = scores.reshape(row_count, local_heads, span_len) * scale
-    own_key = new_keys.astype(jnp.float32).reshape(row_count, local_kv, 1, HEAD_DIM)
-    own_score = (
-        jnp.sum(query_heads.astype(jnp.float32) * own_key, axis=-1).reshape(row_count, local_heads)
-        * scale
-    )
-    places = jnp.arange(span_len, dtype=jnp.int32)
-    at_last = (places[None, :] == (lengths - 1)[:, None]).astype(jnp.float32)
-    last_cum = jnp.sum(cache_logcum * at_last[:, None, :], axis=2)
-    shift = (last_cum + new_log_gate)[:, :, None] - cache_logcum
-    valid = (places[None, :] < lengths[:, None])[:, None, :]
-    past = jnp.where(valid, scores + shift, MASKED)
-    peak = jnp.maximum(jnp.max(past, axis=-1), own_score)
-    past_exp = jnp.exp(past - peak[:, :, None])
-    own_exp = jnp.exp(own_score - peak)
-    total = jnp.sum(past_exp, axis=-1) + own_exp
-    past_weight = (
-        (past_exp / total[:, :, None])
-        .astype(jnp.bfloat16)
-        .reshape(row_count, local_kv, group, span_len)
-    )
-    own_weight = (
-        (own_exp / total)
-        .astype(jnp.bfloat16)
-        .astype(jnp.float32)
-        .reshape(row_count, local_kv, group)
-    )
-    mixed = jnp.einsum(
-        "bkgl,bkdl->bkgd", past_weight, value_heads, preferred_element_type=jnp.float32
-    )
-    own_value = new_values.astype(jnp.float32).reshape(row_count, local_kv, 1, HEAD_DIM)
-    mixed = mixed + own_weight[:, :, :, None] * own_value
-    heads_out = mixed.astype(jnp.bfloat16).reshape(row_count, query_cols)
-    partial_mix = (
-        jnp.dot(heads_out, w_out, preferred_element_type=jnp.float32)
-        .astype(jnp.bfloat16)
-        .astype(jnp.float32)
-    )
-    if dense:
+        new_log_gate = gate_rows.T
         chosen = (routes[:, :, None] == jnp.arange(expert_count, dtype=jnp.int32)).astype(F32)
         weights = jnp.sum(chosen * route_weights[:, :, None], axis=1)
         upper = weights.astype(BF16)
@@ -462,16 +686,13 @@
         lanes = 128
         weights = jnp.concatenate((upper, lower), axis=1)
         weights = jnp.pad(weights, ((0, 0), (0, lanes - weights.shape[1])))
-        pieces = model_width // (2 * chunk)
-        mixed_res, rows_all, weights_all = communicate(
+        rows_all, weights_all = communicate(
             functools.partial(dispatch_kernel, devices, pieces),
             (
-                jax.ShapeDtypeStruct((row_count, model_width), F32),
                 jax.ShapeDtypeStruct((devices, row_count, model_width), BF16),
                 jax.ShapeDtypeStruct((devices, row_count, lanes), BF16),
             ),
             [
-                VMEM((row_count, model_width), BF16),
                 dma((2,)),
                 dma((2,)),
                 dma((bits, pieces)),
@@ -480,10 +701,7 @@
                 dma((bits,)),
             ],
             2,
-            partial_mix.astype(BF16),
-            tokens,
-            norm_gain_mix.reshape(1, -1),
-            norm_gain_ffn.reshape(1, -1),
+            ffn_in,
             weights,
         )
         flat_rows = rows_all.reshape(devices * row_count, model_width)
@@ -517,6 +735,70 @@
         )
         layer_out = (residual_cols + routed).astype(BF16)
         return (layer_out, new_keys, new_values, new_log_gate)
+    joined = jnp.concatenate(
+        (
+            lax.all_gather(w_query, "ep", axis=0, tiled=True),
+            lax.all_gather(w_key, "ep", axis=0, tiled=True),
+            lax.all_gather(w_value, "ep", axis=0, tiled=True),
+        ),
+        axis=1,
+    )
+    projected = jnp.dot(normed, joined, preferred_element_type=jnp.float32)
+    query = projected[:, :query_cols].astype(jnp.bfloat16)
+    new_keys = projected[:, query_cols : query_cols + key_cols].astype(jnp.bfloat16)
+    new_values = projected[:, query_cols + key_cols :].astype(jnp.bfloat16)
+    new_log_gate = jax.nn.log_sigmoid(
+        jnp.dot(normed, w_forget, preferred_element_type=jnp.float32) + forget_bias
+    )
+    local_heads = query_cols // HEAD_DIM
+    local_kv = key_cols // HEAD_DIM
+    group = HEAD_TOTAL // KV_HEADS
+    span_len = cache_keys.shape[2]
+    scale = HEAD_DIM ** (-0.5)
+    query_heads = query.reshape(row_count, local_kv, group, HEAD_DIM)
+    key_heads = cache_keys.reshape(row_count, local_kv, HEAD_DIM, span_len)
+    value_heads = cache_values.reshape(row_count, local_kv, HEAD_DIM, span_len)
+    scores = jnp.einsum(
+        "bkgd,bkdl->bkgl", query_heads, key_heads, preferred_element_type=jnp.float32
+    )
+    scores = scores.reshape(row_count, local_heads, span_len) * scale
+    own_key = new_keys.astype(jnp.float32).reshape(row_count, local_kv, 1, HEAD_DIM)
+    own_score = (
+        jnp.sum(query_heads.astype(jnp.float32) * own_key, axis=-1).reshape(row_count, local_heads)
+        * scale
+    )
+    places = jnp.arange(span_len, dtype=jnp.int32)
+    at_last = (places[None, :] == (lengths - 1)[:, None]).astype(jnp.float32)
+    last_cum = jnp.sum(cache_logcum * at_last[:, None, :], axis=2)
+    shift = (last_cum + new_log_gate)[:, :, None] - cache_logcum
+    valid = (places[None, :] < lengths[:, None])[:, None, :]
+    past = jnp.where(valid, scores + shift, MASKED)
+    peak = jnp.maximum(jnp.max(past, axis=-1), own_score)
+    past_exp = jnp.exp(past - peak[:, :, None])
+    own_exp = jnp.exp(own_score - peak)
+    total = jnp.sum(past_exp, axis=-1) + own_exp
+    past_weight = (
+        (past_exp / total[:, :, None])
+        .astype(jnp.bfloat16)
+        .reshape(row_count, local_kv, group, span_len)
+    )
+    own_weight = (
+        (own_exp / total)
+        .astype(jnp.bfloat16)
+        .astype(jnp.float32)
+        .reshape(row_count, local_kv, group)
+    )
+    mixed = jnp.einsum(
+        "bkgl,bkdl->bkgd", past_weight, value_heads, preferred_element_type=jnp.float32
+    )
+    own_value = new_values.astype(jnp.float32).reshape(row_count, local_kv, 1, HEAD_DIM)
+    mixed = mixed + own_weight[:, :, :, None] * own_value
+    heads_out = mixed.astype(jnp.bfloat16).reshape(row_count, query_cols)
+    partial_mix = (
+        jnp.dot(heads_out, w_out, preferred_element_type=jnp.float32)
+        .astype(jnp.bfloat16)
+        .astype(jnp.float32)
+    )
     mix = lax.psum(partial_mix.astype(jnp.bfloat16), "tp").astype(jnp.float32)
     mixed_res = residual + rms_scaled(mix, norm_gain_mix)
     ffn_in = rms_scaled(mixed_res, norm_gain_ffn).astype(jnp.bfloat16)

time: 121 us -> 105 us (0.87)
  matrix products: 26.3 us -> 9.5 us
  other arithmetic: 9.38 us -> 1.67 us
  local copies, waits for them, and re-layouts: 6.63 us -> 14.1 us
  Pallas kernels: 77.4 us -> 78.9 us
    dot_general x4 -> x0, matrix products: 16.8 us -> none  [the longest x1 6.56 us: body(): jnp.einsum('bkgd,bkdl->bkgl', query_heads, key_heads, preferred_element_t...]
    unnamed x26 -> x31, local copies, waits for them, and re-layouts: 5.45 us -> 13.9 us
    reduce_sum x4 -> x0, other arithmetic: 5.16 us -> none  [the longest x1 2.03 us: body(): total = jnp.sum(past_exp, axis=-1) + own_exp]
    pallas_call x3, Pallas kernels: 77.4 us -> 78.9 us  [communicate(): pl.pallas_call(kernel, out_shape=out_shape, in_specs=[pl.BlockSpec(memory...]
where the time goes in v1:
time: 105 us
  Pallas kernels  78.9 us (75%)
  local copies, waits for them, and re-layouts  14.1 us (13%)
  matrix products  9.5 us (9%)
  other arithmetic  1.67 us (2%)
    pallas_call x3, Pallas kernels, communicate(): pl.pallas_call(kernel, out_shape=out_shape, in_specs=[pl.BlockSpec(memory...  78.9 us
    unnamed x31, local copies, waits for them, and re-layouts  13.9 us
    dot_general x1, matrix products, body(): expert_part = jnp.dot(hidden, expert_down, preferred_element_type=F32)  6.03 us
    dot_general x1, matrix products, body(): gate_part = jnp.dot(flat_rows, expert_gate, preferred_element_type=F32)  3.47 us

profile of v1, /device:TPU:0, one launch (start us, length us, event | category | flops | bytes accessed | tf_op | source)
XLA Modules:
  0.0 104.9 jit_solution(14837914507365001639)
XLA Ops:
  0.6 0.0 copy-start
  0.7 0.9 select_reduce_fusion
  1.5 0.1 copy.28
  1.6 0.0 copy-start.1
  1.7 1.6 %copy-done.1 = f32[32,16,1024]{2,1,0:T(8,128)S(1)} copy-done((f32[32,16,1024]{2,1,0:T(8,128)S(1)}, f32[32,16,1024]{2,1,0:T(8,128)}, u32[]{:S(2)}) %copy-start.1) | copy-done | bytes 2097176
  3.2 0.0 copy-start.3
  3.2 0.9 copy-done.3
  4.2 0.0 copy-start.4
  4.2 0.9 copy-done.4
  5.1 0.8 copy-done.5
  5.9 0.8 copy-done.6
  6.7 0.8 copy-done.7
  7.5 0.7 copy-done.8
  8.2 0.7 copy-done.9
  8.9 0.7 copy-done.10
  9.5 0.7 copy-done.11
  10.2 0.7 copy-done.12
  10.9 31.4 %shard_map.210 = (bf16[32,128]{1,0:T(8,128)(2,1)S(1)}, bf16[32,128]{1,0:T(8,128)(2,1)S(1)}, f32[16,32]{1,0:T(8,128)S(1)}, f32[32,2048]{1,0:T(8,128)S(1)}, bf16[32,2048]{1,0:T(8,128)(2,1)S(1)}) custom-call(bf16[32,2048]{1,0:T(8,128)(2,1)S(1)} %copy-done.4, f32[1,2048]{1,0:T(1,128)S(1)} %bitcast.14, bf16[128,1024]{1,0:T(8,128)(2,1)S(1)} %copy-done.3, ...), custom_call_target="tpu_custom_call" | custom-call | tf_op jit(solution)/shard_map/pallas_call | solution.py:546
  42.2 20.3 %shard_map.211 = (bf16[16,32,2048]{2,1,0:T(8,128)(2,1)S(1)}, bf16[16,32,128]{2,1,0:T(8,128)(2,1)S(1)}) custom-call(bf16[32,2048]{1,0:T(8,128)(2,1)S(1)} %get-tuple-element.12.rows_ref, bf16[32,128]{1,0:T(8,128)(2,1)S(1)} %pad.4.wts_ref), custom_call_target="tpu_custom_call" | custom-call | tf_op jit(solution)/shard_map/pallas_call | solution.py:546
  62.6 0.0 copy-start.13
  62.6 1.3 %copy-done.13 = bf16[16,32,2048]{2,1,0:T(8,128)(2,1)} copy-done((bf16[16,32,2048]{2,1,0:T(8,128)(2,1)}, bf16[16,32,2048]{2,1,0:T(8,128)(2,1)S(1)}, u32[]{:S(2)}) %copy-start.13) | copy-done | bytes 2097176
  63.9 0.1 multiply_reduce_fusion
  64.1 0.1 mul.43
  64.1 3.5 %fusion.3 = f32[512,512]{1,0:T(8,128)S(1)} fusion(bf16[512,2048]{1,0:T(8,128)(2,1)} %bitcast.18, bf16[2048,512]{1,0:T(8,128)(2,1)} %param.33), kind=kOutput, calls=%fused_computation.12 | convolution fusion | flops 1073741824 | bytes 5242880 | tf_op jit(solution)/shard_map/dot_general | solution.py:708
  67.6 0.0 copy-done
  67.6 6.0 %multiply_convert_fusion = bf16[512,2048]{1,0:T(8,128)(2,1)} fusion(bf16[512,2048]{1,0:T(8,128)(2,1)S(1)} %copy-done, f32[512]{0:T(512)S(1)} %mul.43, bf16[512,2048]{1,0:T(8,128)(2,1)} %bitcast.19, bf16[2048,512]{1,0:T(8,128)(2,1)} %param.34, f32[512,512]{1,0:T(8,128)S(1)} %fusion.3), kind=kOutput, calls=%fused_computation | convolution fusion | flops 2151153664 | bytes 9439232 | tf_op jit(solution)/shard_map/dot_general | solution.py:711
  73.7 1.6 %copy-done.2 = bf16[512,2048]{1,0:T(8,128)(2,1)S(1)} copy-done((bf16[512,2048]{1,0:T(8,128)(2,1)S(1)}, bf16[512,2048]{1,0:T(8,128)(2,1)}, u32[]{:S(2)}) %copy-start.2) | copy-done | bytes 2097176
  75.2 27.2 %shard_map.212 = f32[32,1024]{1,0:T(8,128)S(1)} custom-call(bf16[16,32,2048]{2,1,0:T(8,128)(2,1)S(1)} %bitcast.12), custom_call_target="tpu_custom_call" | custom-call | tf_op jit(solution)/shard_map/pallas_call | solution.py:546
  102.4 0.7 add_convert_fusion
  103.1 0.6 copy.32
  103.7 0.6 copy.33
  104.3 0.6 copy.34
  (13 shorter events, 0.0 us)
Async XLA Ops:
  0.6 67.0 %copy-start = (bf16[512,2048]{1,0:T(8,128)(2,1)S(1)}, bf16[512,2048]{1,0:T(8,128)(2,1)}, u32[]{:S(2)}) copy-start(bf16[512,2048]{1,0:T(8,128)(2,1)} %param.35) | copy-start | bytes 6291460
  1.6 1.6 %copy-start.1 = (f32[32,16,1024]{2,1,0:T(8,128)S(1)}, f32[32,16,1024]{2,1,0:T(8,128)}, u32[]{:S(2)}) copy-start(f32[32,16,1024]{2,1,0:T(8,128)} %cum_hbm.1) | copy-start | bytes 6291460
  3.2 0.9 copy-start.3
  4.2 0.9 copy-start.4
  5.1 0.8 copy-start.5
  5.9 0.8 copy-start.6
  6.7 0.8 copy-start.7
  7.5 0.7 copy-start.8
  8.2 0.7 copy-start.9
  8.8 0.7 copy-start.10
  9.5 0.7 copy-start.11
  10.2 0.7 copy-start.12
  62.6 1.3 %copy-start.13 = (bf16[16,32,2048]{2,1,0:T(8,128)(2,1)}, bf16[16,32,2048]{2,1,0:T(8,128)(2,1)S(1)}, u32[]{:S(2)}) copy-start(bf16[16,32,2048]{2,1,0:T(8,128)(2,1)S(1)} %get-tuple-element.13) | copy-start | bytes 6291460
  73.7 1.6 %copy-start.2 = (bf16[512,2048]{1,0:T(8,128)(2,1)S(1)}, bf16[512,2048]{1,0:T(8,128)(2,1)}, u32[]{:S(2)}) copy-start(bf16[512,2048]{1,0:T(8,128)(2,1)} %multiply_convert_fusion) | copy-start | bytes 6291460

commit v2 on v1

--- a/solution.py
+++ b/solution.py
@@ -28,29 +28,6 @@
 MESH = pl.DeviceIdType.MESH
 BF16 = jnp.bfloat16
 F32 = jnp.float32
-
-
-def bit_count(devices):
-    return devices.bit_length() - 1
-
-
-def reversed_bits(place, bits):
-    return sum(((place >> b) & 1) << (bits - 1 - b) for b in range(bits))
-
-
-def flipped(me, mask, bits):
-    other = me
-    for b in range(bits):
-        if (mask >> b) & 1:
-            other = other + (1 - 2 * ((me // (1 << b)) % 2)) * (1 << b)
-    return other
-
-
-def greet(partners):
-    barrier = pltpu.get_barrier_semaphore()
-    for partner in partners:
-        pl.semaphore_signal(barrier, inc=1, device_id=partner, device_id_type=MESH)
-    pl.semaphore_wait(barrier, len(partners))
 
 
 def remote(src, dst, send_sem, recv_sem, partner):
@@ -64,12 +41,6 @@
     )
 
 
-def add_into(acc, got, low, high, shift, cols):
-    acc[low:high, :, cols] = (
-        acc[low:high, :, cols].astype(F32) + got[low + shift : high + shift, :, cols].astype(F32)
-    ).astype(BF16)
-
-
 def copy_of(src, dst, sem):
     return pltpu.make_async_copy(src_ref=src, dst_ref=dst, sem=sem)
 
@@ -78,7 +49,189 @@
     return field * lax.rsqrt(jnp.mean(field * field, axis=-1, keepdims=True) + EPSILON)
 
 
-def front_kernel(
+def expert_part(
+    zs,
+    mixed_res,
+    peers,
+    tp,
+    z,
+    allr,
+    wall,
+    eg,
+    eu,
+    ed,
+    prod,
+    gotc,
+    summed,
+    goty,
+    halves,
+    gotx,
+    both,
+    gotxx,
+    gotyy,
+    outz,
+    gotz,
+    out_ref,
+    sem,
+    arrived,
+):
+    core_peer, x_peer, y_peer, z_peer = peers
+    rows = allr.shape[1] // 4
+    width = allr.shape[2]
+    half = width // 2
+    quarter = half // 2
+    copies = {}
+    slot = [0]
+
+    def send(name, src, dst, peer):
+        n = slot[0]
+        slot[0] += 1
+        copies[name] = remote(src, dst, sem.at[0, n], sem.at[1, n], peer)
+        copies[name].start()
+
+    def block(d, rx, rc):
+        return pl.ds(rc * 2 * rows + rx * rows, rows)
+
+    def side(h):
+        return pl.ds(pl.multiple_of(h * half, half), half)
+
+    def pass_on(name, d, rx, cols, tag):
+        copies[name].wait_recv()
+        send(
+            ("core", d, rx, tag),
+            allr.at[d, block(d, rx, 0), cols],
+            allr.at[d, block(d, rx, 1), cols],
+            core_peer,
+        )
+
+    own = block(0, 0, 0)
+    for d in range(1, zs):
+        send(
+            ("z", d),
+            allr.at[0, own, side(tp)],
+            allr.at[d, own, side(tp)],
+            z_peer(-d),
+        )
+    send(("core", 0, 0, 0), allr.at[0, own], allr.at[0, block(0, 0, 1)], core_peer)
+    send(("x", 0), allr.at[0, own], allr.at[0, block(0, 1, 0)], x_peer)
+    mine, other = side(tp), side(1 - tp)
+    for d in range(1, zs):
+        copies["z", d].wait_recv()
+        for name, peer, rx in (("x", x_peer, 1), ("y0", y_peer, 0)):
+            send(
+                (name, d), allr.at[d, own, mine], allr.at[d, block(d, rx, 0), mine], peer
+            )
+        send(
+            ("core", d, 0, 0),
+            allr.at[d, own, mine],
+            allr.at[d, block(d, 0, 1), mine],
+            core_peer,
+        )
+        if d == 1:
+            pass_on(("x", 0), 0, 1, slice(0, width), 0)
+    for move in arrived:
+        move.wait()
+
+    lane = lax.broadcasted_iota(jnp.int32, wall.shape[1:], 1)
+
+    def expert(d):
+        left = allr[d]
+        gate = jnp.dot(left, eg[...], preferred_element_type=F32)
+        up = jnp.dot(left, eu[...], preferred_element_type=F32)
+        hidden = ((gate / (1.0 + jnp.exp(-gate))) * up).astype(BF16)
+        weight = jnp.sum(jnp.where(lane == z, wall[d], 0.0), axis=1, keepdims=True)
+        for n in range(width // quarter):
+            cols = slice(n * quarter, (n + 1) * quarter)
+            prod[d, :, cols] = (
+                jnp.dot(hidden, ed[:, cols], preferred_element_type=F32) * weight
+            ).astype(BF16)
+        send(("rc", d), prod.at[d, 2 * rows : 4 * rows], gotc.at[d], core_peer)
+
+    def add(a, b):
+        return a.astype(F32) + b.astype(F32)
+
+    def first_sums(d):
+        copies["rc", d].wait_recv()
+        summed[d] = add(prod[d, 0 : 2 * rows, :], gotc[d]).astype(BF16)
+        there = pl.ds(pl.multiple_of((1 - tp) * half, half), quarter)
+        send(("ry", d), summed.at[d, :, there], goty.at[d], y_peer)
+        for h in range(2):
+            send(
+                ("rx", d, h),
+                summed.at[d, rows : 2 * rows, h * half + quarter : (h + 1) * half],
+                gotx.at[d, h],
+                x_peer,
+            )
+
+    def second_sums(d):
+        here = pl.ds(pl.multiple_of(tp * half, half), quarter)
+        copies["ry", d].wait_recv()
+        halves[d] = add(summed[d, :, here], goty[d]).astype(BF16)
+        send(("rxx", d), halves.at[d, rows : 2 * rows], gotxx.at[d], x_peer)
+        for h in range(2):
+            copies["rx", d, h].wait_recv()
+            both[d, h] = add(
+                summed[d, 0:rows, h * half + quarter : (h + 1) * half], gotx[d, h]
+            ).astype(BF16)
+        send(("ryy", d), both.at[d, 1 - tp], gotyy.at[d], y_peer)
+
+    def third_sums(d):
+        copies["rxx", d].wait_recv()
+        low = add(halves[d, 0:rows], gotxx[d])
+        copies["ryy", d].wait_recv()
+        high = add(both[d, tp], gotyy[d])
+        if d == 0:
+            return low, high
+        outz[d, :, 0:quarter] = low.astype(BF16)
+        outz[d, :, quarter:half] = high.astype(BF16)
+        send(("rz", d), outz.at[d], gotz.at[d], z_peer(d))
+
+    copies["core", 0, 0, 0].wait_recv()
+    copies["core", 0, 1, 0].wait_recv()
+    expert(0)
+    for d in range(1, zs):
+        copies["x", d].wait_recv()
+        send(
+            ("y1", d),
+            allr.at[d, block(d, 1, 0), mine],
+            allr.at[d, block(d, 1, 0), mine],
+            y_peer,
+        )
+        send(
+            ("core", d, 1, 0),
+            allr.at[d, block(d, 1, 0), mine],
+            allr.at[d, block(d, 1, 1), mine],
+            core_peer,
+        )
+    first_sums(0)
+    for d in range(1, zs):
+        for rx in range(2):
+            pass_on((f"y{rx}", d), d, rx, other, 1)
+    for step in range(1, zs + 3):
+        if step < zs:
+            for rx in range(2):
+                for tag in range(2):
+                    copies["core", step, rx, tag].wait_recv()
+            expert(step)
+        if 0 < step - 1 < zs:
+            first_sums(step - 1)
+        if 0 <= step - 2 < zs:
+            second_sums(step - 2)
+        if 0 < step - 3 < zs:
+            third_sums(step - 3)
+    low, high = third_sums(0)
+    for d in range(1, zs):
+        copies["rz", d].wait_recv()
+        low = low + gotz[d, :, 0:quarter].astype(F32)
+        high = high + gotz[d, :, quarter:half].astype(F32)
+    for part, value in ((0, low), (quarter, high)):
+        cols = pl.ds(pl.multiple_of(tp * half + part, quarter), quarter)
+        out_ref[:, part : part + quarter] = (mixed_res[:, cols] + value).astype(BF16)
+    for name in copies:
+        copies[name].wait_send()
+
+
+def layer_kernel(
     zs,
     chunk,
     tok_hbm,
@@ -95,11 +248,16 @@
     wo_hbm,
     gmix_hbm,
     gffn_hbm,
+    eg_hbm,
+    eu_hbm,
+    ed_hbm,
+    routes_hbm,
+    shares_hbm,
+    out_ref,
     nk_ref,
     nv_ref,
     gate_ref,
-    res_ref,
-    ffn_ref,
+    mixed_res,
     tok,
     gattn,
     gmix,
@@ -141,6 +299,18 @@
     zrecv,
     ysend,
     yrecv,
+    routes,
+    shares,
+    marks,
+    msend,
+    mrecv,
+    allr,
+    wall,
+    eg,
+    eu,
+    ed,
+    esem,
+    *expert_refs,
 ):
     me, tp = lax.axis_index("ep"), lax.axis_index("tp")
     place = me % SPAN
@@ -175,6 +345,8 @@
         copy_of(len_hbm, lens, local.at[7]),
         copy_of(gmix_hbm, gmix, local.at[8]),
         copy_of(gffn_hbm, gffn, local.at[9]),
+        copy_of(routes_hbm, routes, local.at[14]),
+        copy_of(shares_hbm, shares, local.at[15]),
     ]
     later = [
         copy_of(kc_hbm, kc, local.at[10]),
@@ -182,10 +354,21 @@
         copy_of(cum_hbm, cum, local.at[12]),
         copy_of(wo_hbm, wo, local.at[13]),
     ]
+    last = [
+        copy_of(eg_hbm, eg, local.at[16]),
+        copy_of(eu_hbm, eu, local.at[17]),
+        copy_of(ed_hbm, ed, local.at[18]),
+    ]
     for move in first:
         move.start()
+    others = [(d, rx, rc) for d in range(zs) for rx in range(2) for rc in range(2)][1:]
+
+    def other(d, rx, rc):
+        there = place + rc * (1 - 2 * (me % 2)) + rx * (2 - 4 * ((me // 2) % 2))
+        return (((z - d + zs) % zs) * SPAN + there, tp)
+
+    partners = [other(*key) for key in others] + [y_peer]
     barrier = pltpu.get_barrier_semaphore()
-    partners = [core_peer, x_peer, y_peer] + [z_peer(d) for d in range(1, zs)]
     for partner in partners:
         pl.semaphore_signal(barrier, inc=1, device_id=partner, device_id_type=MESH)
     first[0].wait()
@@ -218,7 +401,7 @@
     view = weights.at[mine]
     direct = remote(view, view, csend.at[0], crecv.at[0], core_peer)
     direct.start()
-    for move in later:
+    for move in later + last:
         move.start()
 
     for move in first[5:7]:
@@ -230,6 +413,26 @@
     for h in range(heads_here):
         logits = logits + jnp.where(row_of == h, bias[h], 0.0)
     gate_ref[...] = jnp.minimum(logits, 0.0) - jnp.log1p(jnp.exp(-jnp.abs(logits)))
+
+    for move in first[10:12]:
+        move.wait()
+    square = lax.broadcasted_iota(jnp.int32, (rows, rows), 0) == lax.broadcasted_iota(
+        jnp.int32, (rows, rows), 1
+    )
+    mark_lane = lax.broadcasted_iota(jnp.int32, marks.shape, 1)
+    value = jnp.zeros(marks.shape, F32)
+    for e in range(zs):
+        line = jnp.sum(jnp.where(routes[...] == e, shares[...], 0.0), axis=0, keepdims=True)
+        column = jnp.sum(jnp.where(square, line, 0.0), axis=1, keepdims=True)
+        value = jnp.where(mark_lane == e, column, value)
+    marks[...] = value
+    wall[0, 0:rows, :] = value
+    tags = {}
+    for n, key in enumerate(others):
+        d, rx, rc = key
+        there = pl.ds(rc * 2 * rows + rx * rows, rows)
+        tags[key] = remote(marks, wall.at[d, there], msend.at[n], mrecv.at[n], other(*key))
+        tags[key].start()
 
     for d in range(1, zs):
         slabs[d].wait_recv()
@@ -368,9 +571,27 @@
     for n in swaps:
         swaps[n].wait_recv()
     mix = part[...].astype(F32) + theirs[...].astype(F32)
-    mixed_res = tok[...].astype(F32) + normalized(mix) * gmix[...]
-    res_ref[...] = mixed_res
-    ffn_ref[...] = (normalized(mixed_res) * gffn[...]).astype(BF16)
+    residual = tok[...].astype(F32) + normalized(mix) * gmix[...]
+    mixed_res[...] = residual
+    allr[0, 0:rows, :] = (normalized(residual) * gffn[...]).astype(BF16)
+    for key in others:
+        tags[key].wait_recv()
+    expert_part(
+        zs,
+        mixed_res,
+        (core_peer, x_peer, y_peer, z_peer),
+        tp,
+        z,
+        allr,
+        wall,
+        eg,
+        eu,
+        ed,
+        *expert_refs,
+        out_ref,
+        esem,
+        last,
+    )
 
     direct.wait_send()
     for k in order:
@@ -382,165 +603,11 @@
         sums[key].wait_send()
     for n in swaps:
         swaps[n].wait_send()
-
-
-def dispatch_kernel(
-    devices,
-    chunks,
-    rows_ref,
-    wts_ref,
-    all_ref,
-    wall_ref,
-    tsend,
-    trecv,
-    send,
-    recv,
-    wsend,
-    wrecv,
-):
-    bits = bit_count(devices)
-    me, tp = lax.axis_index("ep"), lax.axis_index("tp")
-    other_tp = (me, 1 - tp)
-    partners = [(flipped(me, 1 << b, bits), tp) for b in range(bits)]
-    greet(partners + [other_tp])
-    wall_ref[0] = wts_ref[...]
-    all_ref[0] = rows_ref[...]
-    width = all_ref.shape[2] // chunks
-    copies = {}
-    shared = chunks - 2
-    half = 1 << (bits - 1)
-
-    def columns(c):
-        piece = chunks - 2 + tp if c == shared else c
-        return pl.ds(pl.multiple_of(piece * width, width), width)
-
-    def exchange(step, c, cols=None):
-        n = 1 << step
-        partner = partners[bits - 1 - step]
-        if c < chunks:
-            cols = columns(c) if cols is None else cols
-            move = remote(
-                all_ref.at[0:n, :, cols],
-                all_ref.at[n : 2 * n, :, cols],
-                send.at[step, c],
-                recv.at[step, c],
-                partner,
-            )
-        else:
-            move = remote(
-                wall_ref.at[0:n], wall_ref.at[n : 2 * n], wsend.at[step], wrecv.at[step], partner
-            )
-        copies[step, c] = move
-        move.start()
-
-    order = [shared] + list(range(shared)) + [chunks]
-    for step in range(bits - 1):
-        for c in order:
-            if step:
-                copies[step - 1, c].wait_recv()
-            exchange(step, c)
-    copies[bits - 2, shared].wait_recv()
-    across = remote(
-        all_ref.at[1:half, :, columns(shared)],
-        all_ref.at[1:half, :, columns(shared)],
-        tsend.at[1],
-        trecv.at[1],
-        other_tp,
-    )
-    across.start()
-    exchange(bits - 1, shared)
-    for c in order[1:]:
-        copies[bits - 2, c].wait_recv()
-        exchange(bits - 1, c)
-    across.wait_recv()
-    theirs_cols = pl.ds(pl.multiple_of((chunks - 1 - tp) * width, width), width)
-    exchange(bits - 1, chunks - 1, theirs_cols)
-    for c in order + [chunks - 1]:
-        copies[bits - 1, c].wait_recv()
-    across.wait_send()
-    for key in copies:
-        copies[key].wait_send()
-
-
-def combine_kernel(devices, chunk, acc_in, out_ref, acc, got0, got1, got, send, recv):
-    bits = bit_count(devices)
-    me, tp = lax.axis_index("ep"), lax.axis_index("tp")
-    partners = [(flipped(me, 1 << b, bits), tp) for b in range(bits)]
-    other_tp = (me, 1 - tp)
-    greet(partners + [other_tp])
-    half = devices // 2
-    share = acc.shape[2]
-    chunks = share // chunk
-    copies = {}
-
-    def ds(side, c):
-        return pl.ds(pl.multiple_of(side * share + c * chunk, 128), chunk)
-
-    for side in range(2):
-        for c in range(chunks):
-            where = ds(1 - tp, c) if side == 0 else ds(tp, c)
-            copies[0, side, c] = remote(
-                acc_in.at[half:devices, :, where],
-                got0.at[side, :, :, pl.ds(c * chunk, chunk)],
-                send.at[side, c],
-                recv.at[side, c],
-                partners[0],
-            )
-            copies[0, side, c].start()
-    outgoing = got1.at[0]
-    incoming = got1.at[1]
-    for c in range(chunks):
-        cols = slice(c * chunk, (c + 1) * chunk)
-        copies[0, 0, c].wait_recv()
-        outgoing[:, :, cols] = (
-            acc_in[0:half, :, ds(1 - tp, c)].astype(F32) + got0[0, :, :, cols].astype(F32)
-        ).astype(BF16)
-        copies[1, 0, c] = remote(
-            outgoing.at[:, :, pl.ds(c * chunk, chunk)],
-            incoming.at[:, :, pl.ds(c * chunk, chunk)],
-            send.at[2, c],
-            recv.at[2, c],
-            other_tp,
-        )
-        copies[1, 0, c].start()
-    for c in range(chunks):
-        cols = slice(c * chunk, (c + 1) * chunk)
-        copies[0, 1, c].wait_recv()
-        acc[:, :, cols] = (
-            acc_in[0:half, :, ds(tp, c)].astype(F32) + got0[1, :, :, cols].astype(F32)
-        ).astype(BF16)
-
-    def exchange(step, c):
-        n = half >> step
-        copies[step + 1, 0, c] = remote(
-            acc.at[n : 2 * n, :, pl.ds(c * chunk, chunk)],
-            got.at[n : 2 * n, :, pl.ds(c * chunk, chunk)],
-            send.at[step + 2, c],
-            recv.at[step + 2, c],
-            partners[step],
-        )
-        copies[step + 1, 0, c].start()
-
-    for step in range(bits):
-        n = half >> step
-        source = incoming if step == 0 else got
-        shift = 0 if step == 0 else n
-        for c in range(chunks):
-            copies[step + 1, 0, c].wait_recv()
-            cols = slice(c * chunk, (c + 1) * chunk)
-            if step + 1 < bits:
-                add_into(acc, source, n // 2, n, shift, cols)
-                exchange(step + 1, c)
-                add_into(acc, source, 0, n // 2, shift, cols)
-            else:
-                out_ref[:, cols] = acc[0, :, cols].astype(F32) + source[
-                    shift, :, cols
-                ].astype(F32)
-    for key in copies:
-        copies[key].wait_send()
-
-
-def communicate(kernel, out_shape, scratch, number, *operands, places=VMEM):
+    for key in others:
+        tags[key].wait_send()
+
+
+def communicate(kernel, out_shape, scratch, number, *operands, places=VMEM, limit=50):
     whole = pl.BlockSpec(memory_space=VMEM)
     many = isinstance(out_shape, tuple)
     return pl.pallas_call(
@@ -550,7 +617,7 @@
         out_specs=(whole,) * len(out_shape) if many else whole,
         scratch_shapes=scratch,
         compiler_params=pltpu.CompilerParams(
-            collective_id=number, has_side_effects=True, vmem_limit_bytes=50 * 1024 * 1024
+            collective_id=number, has_side_effects=True, vmem_limit_bytes=limit * 1024 * 1024
         ),
     )(*operands)
 
@@ -601,7 +668,6 @@
         and model_width % (2 * chunk) == 0
     )
     if dense:
-        bits = bit_count(devices)
         dma = pltpu.SemaphoreType.DMA
         zs = devices // SPAN
         chunks = joint_cols // chunk
@@ -609,16 +675,17 @@
         strips = row_count * heads_here
         smem = pltpu.SMEM
         pieces = model_width // (2 * chunk)
-        new_keys, new_values, gate_rows, mixed_res, ffn_in = communicate(
-            functools.partial(front_kernel, zs, chunk),
+        half = model_width // 2
+        layer_out, new_keys, new_values, gate_rows = communicate(
+            functools.partial(layer_kernel, zs, chunk),
             (
+                jax.ShapeDtypeStruct((row_count, half), BF16),
                 jax.ShapeDtypeStruct((row_count, key_cols), BF16),
                 jax.ShapeDtypeStruct((row_count, key_cols), BF16),
                 jax.ShapeDtypeStruct((heads_here, row_count), F32),
-                jax.ShapeDtypeStruct((row_count, model_width), F32),
-                jax.ShapeDtypeStruct((row_count, model_width), BF16),
             ),
             [
+                VMEM((row_count, model_width), F32),
                 VMEM((row_count, model_width), BF16),
                 VMEM((1, model_width), F32),
                 VMEM((1, model_width), F32),
@@ -647,7 +714,7 @@
                 VMEM((row_count, query_cols), BF16),
                 VMEM((row_count, model_width), BF16),
                 VMEM((row_count, model_width), BF16),
-                dma((14,)),
+                dma((19,)),
                 dma((chunks,)),
                 dma((chunks,)),
                 dma((1,)),
@@ -660,6 +727,28 @@
                 dma((chunks, zs)),
                 dma((pieces,)),
                 dma((pieces,)),
+                VMEM((TOP, row_count), jnp.int32),
+                VMEM((TOP, row_count), F32),
+                VMEM((row_count, 128), F32),
+                dma((devices,)),
+                dma((devices,)),
+                VMEM((zs, SPAN * row_count, model_width), BF16),
+                VMEM((zs, SPAN * row_count, 128), F32),
+                VMEM(expert_gate.shape, BF16),
+                VMEM(expert_up.shape, BF16),
+                VMEM(expert_down.shape, BF16),
+                dma((2, zs * SPAN * SPAN)),
+                VMEM((zs, SPAN * row_count, model_width), BF16),
+                VMEM((zs, 2 * row_count, model_width), BF16),
+                VMEM((zs, 2 * row_count, model_width), BF16),
+                VMEM((zs, 2 * row_count, half // 2), BF16),
+                VMEM((zs, 2 * row_count, half // 2), BF16),
+                VMEM((zs, 2, row_count, half // 2), BF16),
+                VMEM((zs, 2, row_count, half // 2), BF16),
+                VMEM((zs, row_count, half // 2), BF16),
+                VMEM((zs, row_count, half // 2), BF16),
+                VMEM((zs, row_count, half), BF16),
+                VMEM((zs, row_count, half), BF16),
             ],
             1,
             tokens,
@@ -676,65 +765,15 @@
             w_out,
             norm_gain_mix.reshape(1, -1),
             norm_gain_ffn.reshape(1, -1),
+            expert_gate,
+            expert_up,
+            expert_down,
+            routes.T,
+            route_weights.T,
             places=pl.ANY,
+            limit=63,
         )
-        new_log_gate = gate_rows.T
-        chosen = (routes[:, :, None] == jnp.arange(expert_count, dtype=jnp.int32)).astype(F32)
-        weights = jnp.sum(chosen * route_weights[:, :, None], axis=1)
-        upper = weights.astype(BF16)
-        lower = (weights - upper.astype(F32)).astype(BF16)
-        lanes = 128
-        weights = jnp.concatenate((upper, lower), axis=1)
-        weights = jnp.pad(weights, ((0, 0), (0, lanes - weights.shape[1])))
-        rows_all, weights_all = communicate(
-            functools.partial(dispatch_kernel, devices, pieces),
-            (
-                jax.ShapeDtypeStruct((devices, row_count, model_width), BF16),
-                jax.ShapeDtypeStruct((devices, row_count, lanes), BF16),
-            ),
-            [
-                dma((2,)),
-                dma((2,)),
-                dma((bits, pieces)),
-                dma((bits, pieces)),
-                dma((bits,)),
-                dma((bits,)),
-            ],
-            2,
-            ffn_in,
-            weights,
-        )
-        flat_rows = rows_all.reshape(devices * row_count, model_width)
-        gate_part = jnp.dot(flat_rows, expert_gate, preferred_element_type=F32)
-        up_part = jnp.dot(flat_rows, expert_up, preferred_element_type=F32)
-        hidden = (jax.nn.silu(gate_part) * up_part).astype(BF16)
-        expert_part = jnp.dot(hidden, expert_down, preferred_element_type=F32)
-        mine = lax.axis_index("ep") // SPAN
-        lane = jnp.arange(lanes, dtype=jnp.int32)
-        picked = ((lane == mine) | (lane == mine + expert_count)).astype(F32)
-        own_weight = jnp.sum(weights_all.astype(F32) * picked, axis=2).reshape(-1, 1)
-        share = model_width // 2
-        part = (expert_part * own_weight).astype(BF16)
-        half = devices // 2
-        routed = communicate(
-            functools.partial(combine_kernel, devices, chunk),
-            jax.ShapeDtypeStruct((row_count, share), F32),
-            [
-                VMEM((half, row_count, share), BF16),
-                VMEM((2, half, row_count, share), BF16),
-                VMEM((2, half, row_count, share), BF16),
-                VMEM((half, row_count, share), BF16),
-                dma((bits + 2, share // chunk)),
-                dma((bits + 2, share // chunk)),
-            ],
-            3,
-            part.reshape(devices, row_count, model_width),
-        )
-        residual_cols = lax.dynamic_slice_in_dim(
-            mixed_res, lax.axis_index("tp") * share, share, 1
-        )
-        layer_out = (residual_cols + routed).astype(BF16)
-        return (layer_out, new_keys, new_values, new_log_gate)
+        return (layer_out, new_keys, new_values, gate_rows.T)
     joined = jnp.concatenate(
         (
             lax.all_gather(w_query, "ep", axis=0, tiled=True),

time: 105 us -> 74.9 us (0.71)
  Pallas kernels: 78.9 us -> 68.6 us
  matrix products: 9.5 us -> 0 us
  local copies, waits for them, and re-layouts: 14.1 us -> 5.36 us
  other arithmetic: 1.67 us -> 0 us
    pallas_call x3 -> x1, Pallas kernels: 78.9 us -> 68.6 us  [communicate(): pl.pallas_call(kernel, out_shape=out_shape, in_specs=[pl.BlockSpec(memory...]
    dot_general x2 -> x0, matrix products: 9.5 us -> none  [the longest x1 6.03 us: body(): expert_part = jnp.dot(hidden, expert_down, preferred_element_type=F32)]
    unnamed x31 -> x4, local copies, waits for them, and re-layouts: 13.9 us -> 5.36 us
where the time goes in v2:
time: 74.9 us; the launch traced here: 74.6 us
  Pallas kernels  68.6 us (92%)
  local copies, waits for them, and re-layouts  5.36 us (7%)
    pallas_call x1, Pallas kernels, communicate(): pl.pallas_call(kernel, out_shape=out_shape, in_specs=[pl.BlockSpec(memory...  68.6 us
    unnamed x4, local copies, waits for them, and re-layouts  5.36 us

profile of v2, /device:TPU:0, one launch (start us, length us, event | category | flops | bytes accessed | tf_op | source)
XLA Modules:
  0.0 74.6 jit_solution(8729147387281331994)
XLA Ops:
  0.6 68.6 %shard_map.210 = (bf16[32,1024]{1,0:T(8,128)(2,1)}, bf16[32,128]{1,0:T(8,128)(2,1)}, bf16[32,128]{1,0:T(8,128)(2,1)}, f32[16,32]{1,0:T(8,128)}) custom-call(bf16[32,2048]{1,0:T(8,128)(2,1)} %tok_hbm.1, f32[1,2048]{1,0:T(1,128)} %bitcast.8, bf16[128,1024]{1,0:T(8,128)(2,1)} %wq_hbm.1, bf16[128,128]{1,0:T(8,128)(2,1)} %wk_hbm.1, bf16[128,128]{1,0:T(8,128)(2,1)} %wv_hbm.1, ...), custom_call_target="tpu_custom_call" | custom-call | tf_op jit(solution)/shard_map/pallas_call | solution.py:613
  69.2 1.5 %copy.27 = bf16[32,1024]{1,0:T(8,128)(2,1)} copy(bf16[32,1024]{1,0:T(8,128)(2,1)} %get-tuple-element.16) | data formatting | bytes 131072
  70.7 1.3 %copy.28 = bf16[32,128]{1,0:T(8,128)(2,1)} copy(bf16[32,128]{1,0:T(8,128)(2,1)} %get-tuple-element.17) | data formatting | bytes 16384
  72.0 1.3 %copy.29 = bf16[32,128]{1,0:T(8,128)(2,1)} copy(bf16[32,128]{1,0:T(8,128)(2,1)} %get-tuple-element.18) | data formatting | bytes 16384
  73.3 1.3 %copy.30 = f32[32,16]{0,1:T(8,128)} copy(f32[32,16]{0,1:T(8,128)} %bitcast.11) | data formatting | bytes 4096

commit v3 on v2

v3 whole, which is shorter than its diff:
```python
import functools

import jax
import jax.numpy as jnp
from jax import lax
from jax.experimental import pallas as pl
from jax.experimental.pallas import tpu as pltpu
from jax.sharding import PartitionSpec as P

HEAD_TOTAL = 32
KV_HEADS = 4
HEAD_DIM = 64
SPAN = 4
TOP = 2


EPSILON = 1e-06
MASKED = -1e30
VMEM_LIMIT = 63 * 1024 * 1024


def rms_scaled(field, gain_vector):
    return (
        field * lax.rsqrt(jnp.mean(field * field, axis=-1, keepdims=True) + EPSILON) * gain_vector
    )


VMEM = pltpu.VMEM
MESH = pl.DeviceIdType.MESH
BF16 = jnp.bfloat16
F32 = jnp.float32


def remote(src, dst, send_sem, recv_sem, partner):
    return pltpu.make_async_remote_copy(
        src_ref=src,
        dst_ref=dst,
        send_sem=send_sem,
        recv_sem=recv_sem,
        device_id=partner,
        device_id_type=MESH,
    )


def copy_of(src, dst, sem):
    return pltpu.make_async_copy(src_ref=src, dst_ref=dst, sem=sem)


def taken(ref, sem):
    copy_of(ref, ref, sem).wait()


def normalized(field):
    return field * lax.rsqrt(jnp.mean(field * field, axis=-1, keepdims=True) + EPSILON)


def add(a, b):
    return a.astype(F32) + b.astype(F32)


def expert_part(
    zs,
    at,
    gauge,
    mixed_res,
    peers,
    tp,
    z,
    allr,
    wall,
    eg,
    eu,
    ed,
    weights_here,
    prod,
    gotc,
    summed,
    goty,
    halves,
    gotx,
    both,
    gotxx,
    gotyy,
    outz,
    gotz,
    out_ref,
):
    core_peer, x_peer, y_peer, z_peer = peers
    rows = allr.shape[1] // 4
    width = allr.shape[2]
    half = width // 2
    quarter = half // 2
    sent = {"gather": 0, "combine": 0}

    def send(stage, group, src, dst, peer):
        size = 1
        for extent in src.shape:
            size *= extent
        sent[stage] += size
        remote(src, dst, at(stage), at(group), peer).start()

    def block(rx, rc):
        return pl.ds(rc * 2 * rows + rx * rows, rows)

    def side(h):
        return pl.ds(pl.multiple_of(h * half, half), half)

    mine, other = side(tp), side(1 - tp)
    own, beside = block(0, 0), block(1, 0)
    upper, lower = pl.ds(0, 2 * rows), pl.ds(2 * rows, 2 * rows)
    for d in range(1, zs):
        send("gather", ("z", d), allr.at[0, own, mine], allr.at[d, own, mine], z_peer(-d))
    send("gather", ("core", 0), allr.at[0, own], allr.at[0, block(0, 1)], core_peer)
    send("gather", ("x", 0), allr.at[0, own], allr.at[0, beside], x_peer)

    def from_z(d):
        view = allr.at[d, own, mine]
        taken(view, at(("z", d)))
        send("gather", ("x", d), view, allr.at[d, beside, mine], x_peer)
        send("gather", ("y", d), view, view, y_peer)
        send("gather", ("core", d), view, allr.at[d, block(0, 1), mine], core_peer)

    def from_x(d):
        view = allr.at[d, beside, mine] if d else allr.at[0, beside]
        taken(view, at(("x", d)))
        if d:
            send("gather", ("y", d), view, view, y_peer)
            send("gather", ("core", d), view, allr.at[d, block(1, 1), mine], core_peer)
        else:
            send("gather", ("core", 0), view, allr.at[0, block(1, 1)], core_peer)

    def from_y(d):
        view = allr.at[d, upper, other]
        taken(view, at(("y", d)))
        send("gather", ("core", d), view, allr.at[d, lower, other], core_peer)

    lane = lax.broadcasted_iota(jnp.int32, (4 * rows, wall.shape[1]), 1)

    def expert(d):
        taken(allr.at[d, lower], at(("core", d)))
        left = allr[d]
        gate = jnp.dot(left, eg[...], preferred_element_type=F32)
        up = jnp.dot(left, eu[...], preferred_element_type=F32)
        hidden = ((gate / (1.0 + jnp.exp(-gate))) * up).astype(BF16)
        marks = wall[d * 4 * rows : (d + 1) * 4 * rows, :]
        weight = jnp.sum(jnp.where(lane == z, marks, 0.0), axis=1, keepdims=True)
        for n in range(width // quarter):
            cols = slice(n * quarter, (n + 1) * quarter)
            prod[d, :, cols] = (
                jnp.dot(hidden, ed[:, cols], preferred_element_type=F32) * weight
            ).astype(BF16)
        send("combine", ("rc", d), prod.at[d, lower], gotc.at[d], core_peer)

    def first_sums(d):
        taken(gotc.at[d], at(("rc", d)))
        summed[d] = add(prod[d, 0 : 2 * rows, :], gotc[d]).astype(BF16)
        there = pl.ds(pl.multiple_of((1 - tp) * half, half), quarter)
        send("combine", ("ry", d), summed.at[d, :, there], goty.at[d], y_peer)
        for h in range(2):
            send(
                "combine",
                ("rx", d),
                summed.at[d, pl.ds(rows, rows), pl.ds(h * half + quarter, quarter)],
                gotx.at[d, h],
                x_peer,
            )

    def second_sums(d):
        here = pl.ds(pl.multiple_of(tp * half, half), quarter)
        taken(goty.at[d], at(("ry", d)))
        halves[d] = add(summed[d, :, here], goty[d]).astype(BF16)
        send("combine", ("rxx", d), halves.at[d, pl.ds(rows, rows)], gotxx.at[d], x_peer)
        taken(gotx.at[d], at(("rx", d)))
        for h in range(2):
            both[d, h] = add(
                summed[d, 0:rows, h * half + quarter : (h + 1) * half], gotx[d, h]
            ).astype(BF16)
        send("combine", ("ryy", d), both.at[d, 1 - tp], gotyy.at[d], y_peer)

    def third_sums(d):
        taken(gotxx.at[d], at(("rxx", d)))
        low = add(halves[d, 0:rows], gotxx[d])
        taken(gotyy.at[d], at(("ryy", d)))
        high = add(both[d, tp], gotyy[d])
        if d == 0:
            return low, high
        outz[d, :, 0:quarter] = low.astype(BF16)
        outz[d, :, quarter:half] = high.astype(BF16)
        send("combine", "rz", outz.at[d], gotz.at[d], z_peer(d))

    from_z(1)
    from_x(0)
    for d in range(2, zs):
        from_z(d)
        from_x(d - 1)
    weights_here()
    from_x(zs - 1)
    from_y(1)
    expert(0)
    for d in range(1, zs):
        if d + 1 < zs:
            from_y(d + 1)
        expert(d)
        if d > 1:
            first_sums(d - 1)
    second_sums(1)
    first_sums(zs - 1)
    for d in range(2, zs):
        second_sums(d)
        if d == 2:
            first_sums(0)
        third_sums(d - 1)
    second_sums(0)
    third_sums(zs - 1)
    low, high = third_sums(0)
    taken(gotz.at[pl.ds(1, zs - 1)], at("rz"))
    for d in range(1, zs):
        low = low + gotz[d, :, 0:quarter].astype(F32)
        high = high + gotz[d, :, quarter:half].astype(F32)
    for part, value in ((0, low), (quarter, high)):
        cols = pl.ds(pl.multiple_of(tp * half + part, quarter), quarter)
        out_ref[:, part : part + quarter] = (mixed_res[:, cols] + value).astype(BF16)

    def finish():
        for stage in sent:
            units = sent[stage] // (rows * half)
            taken(gauge.at[pl.ds(0, units), pl.ds(0, rows), pl.ds(0, half)], at(stage))

    return finish


def layer_kernel(
    zs,
    chunk,
    limit,
    tok_hbm,
    gain_hbm,
    wq_hbm,
    wk_hbm,
    wv_hbm,
    wf_hbm,
    bias_hbm,
    kc_hbm,
    vc_hbm,
    cum_hbm,
    len_hbm,
    wo_hbm,
    gmix_hbm,
    gffn_hbm,
    eg_hbm,
    eu_hbm,
    ed_hbm,
    routes_hbm,
    shares_hbm,
    out_hbm,
    nk_hbm,
    nv_hbm,
    gate_hbm,
    out_ref,
    new_ref,
    gate_ref,
    mixed_res,
    tok,
    gattn,
    gains,
    weights,
    wf,
    bias,
    kc,
    vc,
    cum,
    lens,
    wo,
    normed,
    xs,
    own,
    acc,
    got,
    qs,
    kn,
    vn,
    scores,
    probs,
    own_exp,
    inverse,
    outs,
    heads,
    part,
    theirs,
    sem,
    routes,
    shares,
    marks,
    allr,
    wall,
    eg,
    eu,
    ed,
    *expert_refs,
):
    me, tp = lax.axis_index("ep"), lax.axis_index("tp")
    place = me % SPAN
    z = me // SPAN
    core_peer = (me + 1 - 2 * (me % 2), tp)
    x_peer = (me + 2 - 4 * ((me // 2) % 2), tp)
    y_peer = (me, 1 - tp)
    numbers = {}

    def at(group):
        number = numbers.setdefault(group, len(numbers))
        assert number < limit
        return sem.at[number]

    def z_peer(d):
        return (((z + d + zs) % zs) * SPAN + place, tp)

    rows, width = tok.shape
    depth = wq_hbm.shape[0]
    query_cols = wq_hbm.shape[1]
    key_cols = wk_hbm.shape[1]
    slab = SPAN * depth
    chunks = weights.shape[0]
    heads_here = query_cols // HEAD_DIM
    mine = pl.ds(pl.multiple_of(place * depth, depth), depth)
    x_place = place + 2 - 4 * ((me // 2) % 2)
    xs_rows = pl.ds(pl.multiple_of(x_place * depth, depth), depth)

    def begin(group, src, dst):
        copy_of(src, dst, at(group)).start()

    begin("tok", tok_hbm, tok)
    begin("gattn", gain_hbm, gattn)
    for k in range(chunks - 1):
        begin("w", wq_hbm.at[:, pl.ds(k * chunk, chunk)], weights.at[k, mine])
    begin("w", wk_hbm, weights.at[chunks - 1, mine, pl.ds(0, key_cols)])
    begin("w", wv_hbm, weights.at[chunks - 1, mine, pl.ds(key_cols, key_cols)])
    begin("wf", wf_hbm, wf)
    begin("bias", bias_hbm, bias)
    begin("lens", len_hbm, lens)
    begin("routes", routes_hbm, routes)
    begin("shares", shares_hbm, shares)
    begin("gains", gmix_hbm, gains.at[0])
    begin("gains", gffn_hbm, gains.at[1])

    others = [(d, rx, rc) for d in range(zs) for rx in range(2) for rc in range(2)][1:]

    def other(d, rx, rc):
        there = place + rc * (1 - 2 * (me % 2)) + rx * (2 - 4 * ((me // 2) % 2))
        return (((z - d + zs) % zs) * SPAN + there, tp)

    partners = [other(*key) for key in others] + [y_peer]
    barrier = pltpu.get_barrier_semaphore()
    for partner in partners:
        pl.semaphore_signal(barrier, inc=1, device_id=partner, device_id_type=MESH)
    taken(tok, at("tok"))
    taken(gattn, at("gattn"))
    normed[...] = (normalized(tok[...].astype(F32)) * gattn[...]).astype(BF16)
    xs[0:rows, :] = normed[:, pl.ds(pl.multiple_of(z * slab, slab), slab)]
    taken(weights.at[:, mine], at("w"))
    pl.semaphore_wait(barrier, len(partners))

    order = [chunks - 1] + list(range(chunks - 1))
    for k in order:
        view = weights.at[k, mine]
        remote(view, view, at("across"), at(("across", k)), x_peer).start()
        if k == order[0]:
            for d in range(1, zs):
                peer = z_peer(d)
                there = pl.ds(pl.multiple_of((peer[0] // SPAN) * slab, slab), slab)
                dst = xs.at[pl.ds(d * rows, rows)]
                remote(normed.at[:, there], dst, at("slabs"), at("slab"), peer).start()
    view = weights.at[:, mine]
    remote(view, view, at("directs"), at("direct"), core_peer).start()
    begin("kc", kc_hbm, kc)
    begin("cum", cum_hbm, cum)
    begin("vc", vc_hbm, vc)
    begin("wo", wo_hbm, wo)
    begin("eg", eg_hbm, eg)
    begin("eu", eu_hbm, eu)
    begin("ed", ed_hbm, ed)

    taken(wf, at("wf"))
    taken(bias, at("bias"))
    logits = lax.dot_general(
        wf[...], normed[...], (((1,), (1,)), ((), ())), preferred_element_type=F32
    )
    row_of = lax.broadcasted_iota(jnp.int32, logits.shape, 0)
    for h in range(heads_here):
        logits = logits + jnp.where(row_of == h, bias[h], 0.0)
    gate_ref[...] = jnp.minimum(logits, 0.0) - jnp.log1p(jnp.exp(-jnp.abs(logits)))

    taken(routes, at("routes"))
    taken(shares, at("shares"))
    square = lax.broadcasted_iota(jnp.int32, (rows, rows), 0) == lax.broadcasted_iota(
        jnp.int32, (rows, rows), 1
    )
    mark_lane = lax.broadcasted_iota(jnp.int32, marks.shape, 1)
    value = jnp.zeros(marks.shape, F32)
    for e in range(zs):
        line = jnp.sum(jnp.where(routes[...] == e, shares[...], 0.0), axis=0, keepdims=True)
        column = jnp.sum(jnp.where(square, line, 0.0), axis=1, keepdims=True)
        value = jnp.where(mark_lane == e, column, value)
    marks[...] = value
    wall[0:rows, :] = value
    for key in others:
        d, rx, rc = key
        there = pl.ds(d * 4 * rows + rc * 2 * rows + rx * rows, rows)
        remote(marks, wall.at[there], at("tags"), at("tag"), other(*key)).start()

    def relay(k):
        view = weights.at[k, xs_rows]
        taken(view, at(("across", k)))
        remote(view, view, at("forwards"), at(("forward", k)), core_peer).start()

    def multiply(k):
        taken(weights.at[k, xs_rows], at(("forward", k)))
        product = jnp.dot(xs[...], weights[k], preferred_element_type=F32)
        own[k] = product[0:rows]
        acc[k] = product[rows:].astype(BF16)
        for d in range(1, zs):
            view = pl.ds((d - 1) * rows, rows)
            remote(acc.at[k, view], got.at[k, view], at("sums"), at(("sum", k)), z_peer(-d)).start()

    relay(order[0])
    relay(order[1])
    taken(xs.at[pl.ds(rows, (zs - 1) * rows)], at("slab"))
    taken(view, at("direct"))
    for n, k in enumerate(order):
        multiply(k)
        if n + 2 < chunks:
            relay(order[n + 2])

    lane = lax.broadcasted_iota(jnp.int32, (rows, 2 * HEAD_DIM), 1)
    low = lane < HEAD_DIM
    group = heads_here // 2

    def collect(k):
        taken(got.at[k], at(("sum", k)))
        value = own[k]
        for d in range(1, zs):
            value = value + got[k, (d - 1) * rows : d * rows, :].astype(F32)
        value = value.astype(BF16)
        if k == order[0]:
            for n, (held, shifted, result) in enumerate(((0, kn, nk_hbm), (1, vn, nv_hbm))):
                piece = value[:, n * key_cols : (n + 1) * key_cols]
                new_ref[held] = piece
                begin("news", new_ref.at[held], result)
                shifted[0] = piece.astype(F32)
                shifted[1] = pltpu.roll(piece.astype(F32), HEAD_DIM, 1)
            begin("gates", gate_ref, gate_hbm)
            return
        value = value.astype(F32) * (HEAD_DIM**-0.5)
        for j in range(chunk // (2 * HEAD_DIM)):
            block = value[:, j * 2 * HEAD_DIM : (j + 1) * 2 * HEAD_DIM]
            kv, head = divmod((k * chunk) // HEAD_DIM + 2 * j, group)
            qs[kv, pl.ds(head, rows, stride=group), :] = block
            qs[kv, pl.ds(head + 1, rows, stride=group), :] = pltpu.roll(block, HEAD_DIM, 1)

    unroll = 8
    turns = rows // unroll
    span_len = cum.shape[2]
    places = lax.broadcasted_iota(jnp.int32, (group, span_len), 1)
    lane_b = lax.broadcasted_iota(jnp.int32, (group, rows), 1)

    def strip(b):
        return pl.ds(pl.multiple_of(b * group, group), group)

    def attend(kv):
        these = slice(kv * group, (kv + 1) * group)
        dims = slice(kv * HEAD_DIM, (kv + 1) * HEAD_DIM)

        def score(g):
            for u in range(unroll):
                b = g * unroll + u
                scores[strip(b), :] = jnp.dot(
                    qs[kv, strip(b), 0:HEAD_DIM].astype(BF16),
                    kc[b, dims, :],
                    preferred_element_type=F32,
                )

        def soften(g):
            for u in range(unroll):
                b = g * unroll + u
                length = lens[b]
                logcum = cum[b, these, :]
                gate = jnp.sum(
                    jnp.where(lane_b == b, gate_ref[these, :], 0.0), axis=1, keepdims=True
                )
                last = jnp.sum(
                    jnp.where(places == length - 1, logcum, 0.0), axis=1, keepdims=True
                )
                mine_score = jnp.sum(
                    qs[kv, strip(b), 0:HEAD_DIM] * kn[kv, pl.ds(b, 1), 0:HEAD_DIM],
                    axis=1,
                    keepdims=True,
                )
                past = scores[strip(b), :] + ((last + gate) - logcum)
                past = jnp.where(places < length, past, MASKED)
                peak = jnp.maximum(jnp.max(past, axis=1, keepdims=True), mine_score)
                raised = jnp.exp(past - peak)
                mine_exp = jnp.exp(mine_score - peak)
                probs[strip(b), :] = raised
                sum_all = jnp.sum(raised, axis=1, keepdims=True) + mine_exp
                own_exp[strip(b), :] = jnp.broadcast_to(mine_exp, (group, HEAD_DIM))
                inverse[strip(b), :] = jnp.broadcast_to(1.0 / sum_all, (group, HEAD_DIM))

        def weigh(g):
            for u in range(unroll):
                b = g * unroll + u
                mixed = lax.dot_general(
                    probs[strip(b), :].astype(BF16),
                    vc[b, dims, :],
                    (((1,), (1,)), ((), ())),
                    preferred_element_type=F32,
                )
                mixed = mixed + own_exp[strip(b), :] * vn[kv, pl.ds(b, 1), 0:HEAD_DIM]
                outs[kv, strip(b), 0:HEAD_DIM] = mixed * inverse[strip(b), :]

        def turn(g, carry):
            weigh(g - 2)
            soften(g - 1)
            score(g)
            return carry

        score(0)
        soften(0)
        score(1)
        lax.fori_loop(2, turns, turn, 0)
        weigh(turns - 2)
        soften(turns - 1)
        weigh(turns - 1)

    per_kv = (chunks - 1) // 2
    for k in order[: 1 + per_kv]:
        collect(k)
    taken(lens, at("lens"))
    taken(kc, at("kc"))
    taken(cum, at("cum"))
    taken(vc, at("vc"))
    attend(0)
    for k in order[1 + per_kv :]:
        collect(k)
    attend(1)

    for m in range(heads_here // 2):
        kv, head = divmod(2 * m, group)
        a = outs[kv, pl.ds(head, rows, stride=group), :]
        b = pltpu.roll(outs[kv, pl.ds(head + 1, rows, stride=group), :], HEAD_DIM, 1)
        heads[:, m * 2 * HEAD_DIM : (m + 1) * 2 * HEAD_DIM] = jnp.where(low, a, b).astype(BF16)

    taken(wo, at("wo"))
    piece = 2 * chunk
    for n in range(width // piece):
        cols = pl.ds(n * piece, piece)
        part[:, cols] = jnp.dot(
            heads[...], wo[:, cols], preferred_element_type=F32
        ).astype(BF16)
        remote(part.at[:, cols], theirs.at[:, cols], at("swaps"), at("swap"), y_peer).start()
    taken(gains, at("gains"))
    taken(theirs, at("swap"))
    mix = part[...].astype(F32) + theirs[...].astype(F32)
    residual = tok[...].astype(F32) + normalized(mix) * gains[0]
    mixed_res[...] = residual
    allr[0, 0:rows, :] = (normalized(residual) * gains[1]).astype(BF16)
    tagged = wall.at[pl.ds(rows, (4 * zs - 1) * rows)]
    taken(tagged, at("tag"))

    def weights_here():
        taken(eg, at("eg"))
        taken(eu, at("eu"))
        taken(ed, at("ed"))

    finish = expert_part(
        zs,
        at,
        kc,
        mixed_res,
        (core_peer, x_peer, y_peer, z_peer),
        tp,
        z,
        allr,
        wall,
        eg,
        eu,
        ed,
        weights_here,
        *expert_refs,
        out_ref,
    )
    begin("out", out_ref, out_hbm)
    finish()
    view = weights.at[:, mine]
    for group in ("across", "directs", "forwards"):
        taken(view, at(group))
    taken(xs.at[pl.ds(rows, (zs - 1) * rows)], at("slabs"))
    taken(got, at("sums"))
    taken(theirs, at("swaps"))
    taken(tagged, at("tags"))
    taken(new_ref, at("news"))
    taken(gate_ref, at("gates"))
    taken(out_ref, at("out"))
    assert len(numbers) == limit, len(numbers)


def communicate(kernel, out_shape, scratch, number, *operands):
    place = pl.BlockSpec(memory_space=pl.ANY)
    return pl.pallas_call(
        kernel,
        out_shape=out_shape,
        in_specs=[place] * len(operands),
        out_specs=(place,) * len(out_shape),
        scratch_shapes=scratch,
        compiler_params=pltpu.CompilerParams(
            collective_id=number, has_side_effects=True, vmem_limit_bytes=VMEM_LIMIT
        ),
    )(*operands)


def deliver_kernel(count, *refs):
    sources, results = refs[:count], refs[count : 2 * count]
    held, sems = refs[2 * count : 3 * count], refs[3 * count]
    moves = [copy_of(sources[n], held[n], sems.at[0, n]) for n in range(count)]
    for move in moves:
        move.start()
    outs = [copy_of(held[n], results[n], sems.at[1, n]) for n in range(count)]
    for move, out in zip(moves, outs):
        move.wait()
        out.start()
    for out in outs:
        out.wait()


def deliver(*arrays):
    count = len(arrays)
    place = pl.BlockSpec(memory_space=pl.ANY)
    return pl.pallas_call(
        functools.partial(deliver_kernel, count),
        out_shape=tuple(jax.ShapeDtypeStruct(a.shape, a.dtype) for a in arrays),
        in_specs=[place] * count,
        out_specs=(place,) * count,
        scratch_shapes=[VMEM(a.shape, a.dtype) for a in arrays]
        + [pltpu.SemaphoreType.DMA((2, count))],
        compiler_params=pltpu.CompilerParams(vmem_limit_bytes=VMEM_LIMIT),
    )(*arrays)


def body(
    tokens,
    norm_gain_attn,
    w_query,
    w_key,
    w_value,
    w_forget,
    forget_bias,
    cache_keys,
    cache_values,
    cache_logcum,
    lengths,
    w_out,
    norm_gain_mix,
    norm_gain_ffn,
    expert_gate,
    expert_up,
    expert_down,
    routes,
    route_weights,
):
    row_count = tokens.shape[0]
    model_width = tokens.shape[1]
    query_cols = w_query.shape[1]
    key_cols = w_key.shape[1]
    residual = tokens.astype(jnp.float32)
    normed = rms_scaled(residual, norm_gain_attn).astype(jnp.bfloat16)
    devices = lax.axis_size("ep")
    expert_count = devices // SPAN
    slot_count = max(2, min(row_count, 2 * row_count * TOP // expert_count))
    depth = w_query.shape[0]
    joint_cols = query_cols + 2 * key_cols
    chunk = 256
    dense = (
        slot_count == row_count
        and lax.axis_size("tp") == 2
        and devices & (devices - 1) == 0
        and depth % 128 == 0
        and joint_cols % chunk == 0
        and devices % SPAN == 0
        and key_cols == 2 * HEAD_DIM
        and 2 * key_cols == chunk
        and row_count % 8 == 0
        and model_width % (2 * chunk) == 0
    )
    if dense:
        dma = pltpu.SemaphoreType.DMA
        zs = devices // SPAN
        chunks = joint_cols // chunk
        heads_here = query_cols // HEAD_DIM
        strips = row_count * heads_here // 2
        sems = 31 + 3 * chunks + 9 * zs
        smem = pltpu.SMEM
        half = model_width // 2
        layer_out, new_keys, new_values, gate_rows = communicate(
            functools.partial(layer_kernel, zs, chunk, sems),
            (
                jax.ShapeDtypeStruct((row_count, half), BF16),
                jax.ShapeDtypeStruct((row_count, key_cols), BF16),
                jax.ShapeDtypeStruct((row_count, key_cols), BF16),
                jax.ShapeDtypeStruct((heads_here, row_count), F32),
            ),
            [
                VMEM((row_count, half), BF16),
                VMEM((2, row_count, key_cols), BF16),
                VMEM((heads_here, row_count), F32),
                VMEM((row_count, model_width), F32),
                VMEM((row_count, model_width), BF16),
                VMEM((1, model_width), F32),
                VMEM((2, 1, model_width), F32),
                VMEM((chunks, SPAN * depth, chunk), BF16),
                VMEM((heads_here, model_width), BF16),
                smem((heads_here,), F32),
                VMEM(cache_keys.shape, BF16),
                VMEM(cache_values.shape, BF16),
                VMEM(cache_logcum.shape, F32),
                smem((row_count,), jnp.int32),
                VMEM(w_out.shape, BF16),
                VMEM((row_count, model_width), BF16),
                VMEM((zs * row_count, SPAN * depth), BF16),
                VMEM((chunks, row_count, chunk), F32),
                VMEM((chunks, (zs - 1) * row_count, chunk), BF16),
                VMEM((chunks, (zs - 1) * row_count, chunk), BF16),
                VMEM((2, strips, key_cols), F32),
                VMEM((2, row_count, key_cols), F32),
                VMEM((2, row_count, key_cols), F32),
                VMEM((strips, cache_keys.shape[2]), F32),
                VMEM((strips, cache_keys.shape[2]), F32),
                VMEM((strips, HEAD_DIM), F32),
                VMEM((strips, HEAD_DIM), F32),
                VMEM((2, strips, key_cols), F32),
                VMEM((row_count, query_cols), BF16),
                VMEM((row_count, model_width), BF16),
                VMEM((row_count, model_width), BF16),
                dma((sems,)),
                VMEM((TOP, row_count), jnp.int32),
                VMEM((TOP, row_count), F32),
                VMEM((row_count, 128), F32),
                VMEM((zs, SPAN * row_count, model_width), BF16),
                VMEM((zs * SPAN * row_count, 128), F32),
                VMEM(expert_gate.shape, BF16),
                VMEM(expert_up.shape, BF16),
                VMEM(expert_down.shape, BF16),
                VMEM((zs, SPAN * row_count, model_width), BF16),
                VMEM((zs, 2 * row_count, model_width), BF16),
                VMEM((zs, 2 * row_count, model_width), BF16),
                VMEM((zs, 2 * row_count, half // 2), BF16),
                VMEM((zs, 2 * row_count, half // 2), BF16),
                VMEM((zs, 2, row_count, half // 2), BF16),
                VMEM((zs, 2, row_count, half // 2), BF16),
                VMEM((zs, row_count, half // 2), BF16),
                VMEM((zs, row_count, half // 2), BF16),
                VMEM((zs, row_count, half), BF16),
                VMEM((zs, row_count, half), BF16),
            ],
            1,
            tokens,
            norm_gain_attn.reshape(1, -1),
            w_query,
            w_key,
            w_value,
            w_forget.T,
            forget_bias,
            cache_keys,
            cache_values,
            cache_logcum,
            lengths,
            w_out,
            norm_gain_mix.reshape(1, -1),
            norm_gain_ffn.reshape(1, -1),
            expert_gate,
            expert_up,
            expert_down,
            routes.T,
            route_weights.T,
        )
        layer_out, new_keys, new_values, gate_rows = deliver(
            layer_out, new_keys, new_values, gate_rows
        )
        return (layer_out, new_keys, new_values, gate_rows.T)
    joined = jnp.concatenate(
        (
            lax.all_gather(w_query, "ep", axis=0, tiled=True),
            lax.all_gather(w_key, "ep", axis=0, tiled=True),
            lax.all_gather(w_value, "ep", axis=0, tiled=True),
        ),
        axis=1,
    )
    projected = jnp.dot(normed, joined, preferred_element_type=jnp.float32)
    query = projected[:, :query_cols].astype(jnp.bfloat16)
    new_keys = projected[:, query_cols : query_cols + key_cols].astype(jnp.bfloat16)
    new_values = projected[:, query_cols + key_cols :].astype(jnp.bfloat16)
    new_log_gate = jax.nn.log_sigmoid(
        jnp.dot(normed, w_forget, preferred_element_type=jnp.float32) + forget_bias
    )
    local_heads = query_cols // HEAD_DIM
    local_kv = key_cols // HEAD_DIM
    group = HEAD_TOTAL // KV_HEADS
    span_len = cache_keys.shape[2]
    scale = HEAD_DIM ** (-0.5)
    query_heads = query.reshape(row_count, local_kv, group, HEAD_DIM)
    key_heads = cache_keys.reshape(row_count, local_kv, HEAD_DIM, span_len)
    value_heads = cache_values.reshape(row_count, local_kv, HEAD_DIM, span_len)
    scores = jnp.einsum(
        "bkgd,bkdl->bkgl", query_heads, key_heads, preferred_element_type=jnp.float32
    )
    scores = scores.reshape(row_count, local_heads, span_len) * scale
    own_key = new_keys.astype(jnp.float32).reshape(row_count, local_kv, 1, HEAD_DIM)
    own_score = (
        jnp.sum(query_heads.astype(jnp.float32) * own_key, axis=-1).reshape(row_count, local_heads)
        * scale
    )
    places = jnp.arange(span_len, dtype=jnp.int32)
    at_last = (places[None, :] == (lengths - 1)[:, None]).astype(jnp.float32)
    last_cum = jnp.sum(cache_logcum * at_last[:, None, :], axis=2)
    shift = (last_cum + new_log_gate)[:, :, None] - cache_logcum
    valid = (places[None, :] < lengths[:, None])[:, None, :]
    past = jnp.where(valid, scores + shift, MASKED)
    peak = jnp.maximum(jnp.max(past, axis=-1), own_score)
    past_exp = jnp.exp(past - peak[:, :, None])
    own_exp = jnp.exp(own_score - peak)
    total = jnp.sum(past_exp, axis=-1) + own_exp
    past_weight = (
        (past_exp / total[:, :, None])
        .astype(jnp.bfloat16)
        .reshape(row_count, local_kv, group, span_len)
    )
    own_weight = (
        (own_exp / total)
        .astype(jnp.bfloat16)
        .astype(jnp.float32)
        .reshape(row_count, local_kv, group)
    )
    mixed = jnp.einsum(
        "bkgl,bkdl->bkgd", past_weight, value_heads, preferred_element_type=jnp.float32
    )
    own_value = new_values.astype(jnp.float32).reshape(row_count, local_kv, 1, HEAD_DIM)
    mixed = mixed + own_weight[:, :, :, None] * own_value
    heads_out = mixed.astype(jnp.bfloat16).reshape(row_count, query_cols)
    partial_mix = (
        jnp.dot(heads_out, w_out, preferred_element_type=jnp.float32)
        .astype(jnp.bfloat16)
        .astype(jnp.float32)
    )
    mix = lax.psum(partial_mix.astype(jnp.bfloat16), "tp").astype(jnp.float32)
    mixed_res = residual + rms_scaled(mix, norm_gain_mix)
    ffn_in = rms_scaled(mixed_res, norm_gain_ffn).astype(jnp.bfloat16)
    flat_routes = routes.reshape(-1)
    expert_hits = (
        flat_routes[:, None] == jnp.arange(expert_count, dtype=jnp.int32)[None, :]
    ).astype(jnp.int32)
    earlier = jnp.cumsum(expert_hits, axis=0) - expert_hits
    slot_index = jnp.sum(earlier * expert_hits, axis=1)
    in_slot = (slot_index[:, None] == jnp.arange(slot_count, dtype=jnp.int32)[None, :]).astype(
        jnp.float32
    )
    placing = expert_hits.astype(jnp.float32)[:, :, None] * in_slot[:, None, :]
    placing = placing.reshape(row_count, TOP, expert_count * slot_count)
    selector = jnp.sum(placing, axis=1).astype(jnp.bfloat16)
    weighing = jnp.sum(placing * route_weights[:, :, None], axis=1)
    packed = jnp.einsum("ra,rd->ad", selector, ffn_in, preferred_element_type=jnp.float32).astype(
        jnp.bfloat16
    )
    outgoing = jnp.broadcast_to(
        packed.reshape(expert_count, 1, slot_count, model_width),
        (expert_count, SPAN, slot_count, model_width),
    )
    outgoing = outgoing.reshape(expert_count * SPAN, slot_count, model_width)
    arrived = lax.all_to_all(outgoing, "ep", split_axis=0, concat_axis=0, tiled=True)
    sources, slots, width = arrived.shape
    flat_rows = arrived.reshape(sources * slots, width)
    gate_part = jnp.dot(flat_rows, expert_gate, preferred_element_type=jnp.float32)
    up_part = jnp.dot(flat_rows, expert_up, preferred_element_type=jnp.float32)
    hidden = (jax.nn.silu(gate_part) * up_part).astype(jnp.bfloat16)
    expert_part = jnp.dot(hidden, expert_down, preferred_element_type=jnp.float32)
    col_share = lax.psum_scatter(
        expert_part.astype(jnp.bfloat16), "tp", scatter_dimension=1, tiled=True
    ).astype(jnp.float32)
    returned = lax.all_to_all(
        col_share.reshape(sources, slots, -1).astype(jnp.bfloat16),
        "ep",
        split_axis=0,
        concat_axis=0,
        tiled=True,
    ).astype(jnp.float32)
    col_width = returned.shape[2]
    per_expert = jnp.sum(returned.reshape(expert_count, SPAN, slot_count, col_width), axis=1)
    per_expert = per_expert.reshape(expert_count * slot_count, col_width)
    routed = jnp.dot(
        weighing, per_expert, precision=lax.Precision.HIGHEST, preferred_element_type=jnp.float32
    )
    col_start = lax.axis_index("tp") * col_width
    residual_cols = lax.dynamic_slice_in_dim(mixed_res, col_start, col_width, 1)
    layer_out = (residual_cols + routed).astype(jnp.bfloat16)
    return (layer_out, new_keys, new_values, new_log_gate)


def solution(mesh):
    placed = (
        P("ep", None),
        P(),
        P("ep", "tp"),
        P("ep", "tp"),
        P("ep", "tp"),
        P(None, "tp"),
        P("tp"),
        P("ep", "tp", None),
        P("ep", "tp", None),
        P("ep", "tp", None),
        P("ep"),
        P("tp", None),
        P(),
        P(),
        P(None, ("ep", "tp")),
        P(None, ("ep", "tp")),
        P(("ep", "tp"), None),
        P("ep", None),
        P("ep", None),
    )
    return jax.shard_map(
        body,
        mesh=mesh,
        in_specs=placed,
        out_specs=(P("ep", "tp"), P("ep", "tp"), P("ep", "tp"), P("ep", "tp")),
        check_vma=False,
    )
```

time: 74.9 us -> 64.9 us (0.87)
  local copies, waits for them, and re-layouts: 5.36 us -> 0 us
  Pallas kernels: 68.6 us -> 64 us
    unnamed x4 -> x0, local copies, waits for them, and re-layouts: 5.36 us -> none
    pallas_call x1 -> x2, Pallas kernels: 68.6 us -> 64 us  [the longest x1 62.5 us: communicate(): pl.pallas_call(kernel, out_shape=out_shape, in_specs=[place] * len(operan...]
where the time goes in v3:
time: 64.9 us; the launch traced here: 64.7 us
  Pallas kernels  64 us (99%)
  between operations  0.65 us (1%)
    pallas_call x1, Pallas kernels, communicate(): pl.pallas_call(kernel, out_shape=out_shape, in_specs=[place] * len(operan...  62.5 us
    pallas_call x1, Pallas kernels, deliver(): pl.pallas_call(functools.partial(deliver_kernel, count), out_shape=tuple(...  1.55 us

profile of v3, /device:TPU:0, one launch (start us, length us, event | category | flops | bytes accessed | tf_op | source)
XLA Modules:
  0.0 64.7 jit_solution(1353384620415823217)
XLA Ops:
  0.6 62.5 %shard_map.210 = (bf16[32,1024]{1,0:T(8,128)(2,1)}, bf16[32,128]{1,0:T(8,128)(2,1)}, bf16[32,128]{1,0:T(8,128)(2,1)}, f32[16,32]{1,0:T(8,128)}) custom-call(bf16[32,2048]{1,0:T(8,128)(2,1)} %tok_hbm.1, f32[1,2048]{1,0:T(1,128)} %bitcast.8, bf16[128,1024]{1,0:T(8,128)(2,1)} %wq_hbm.1, bf16[128,128]{1,0:T(8,128)(2,1)} %wk_hbm.1, bf16[128,128]{1,0:T(8,128)(2,1)} %wv_hbm.1, ...), custom_call_target="tpu_custom_call" | custom-call | tf_op jit(solution)/shard_map/pallas_call | solution.py:607
  63.1 1.5 %shard_map.211 = (bf16[32,1024]{1,0:T(8,128)(2,1)}, bf16[32,128]{1,0:T(8,128)(2,1)}, bf16[32,128]{1,0:T(8,128)(2,1)}, f32[16,32]{1,0:T(8,128)}) custom-call(bf16[32,1024]{1,0:T(8,128)(2,1)} %get-tuple-element.12.refs_0_, bf16[32,128]{1,0:T(8,128)(2,1)} %get-tuple-element.13.refs_1_, bf16[32,128]{1,0:T(8,128)(2,1)} %get-tuple-element.14.refs_2_, ...), custom_call_target="tpu_custom_call" | custom-call | tf_op jit(solution)/shard_map/pallas_call | solution.py:636

commit v4 on v3

--- a/solution.py
+++ b/solution.py
@@ -102,39 +102,52 @@
     def block(rx, rc):
         return pl.ds(rc * 2 * rows + rx * rows, rows)
 
-    def side(h):
-        return pl.ds(pl.multiple_of(h * half, half), half)
-
-    mine, other = side(tp), side(1 - tp)
+    def cols(h, n):
+        return pl.ds(pl.multiple_of(h * half + n * quarter, quarter), quarter)
+
     own, beside = block(0, 0), block(1, 0)
     upper, lower = pl.ds(0, 2 * rows), pl.ds(2 * rows, 2 * rows)
     for d in range(1, zs):
-        send("gather", ("z", d), allr.at[0, own, mine], allr.at[d, own, mine], z_peer(-d))
+        for n in range(2):
+            mine = cols(tp, n)
+            send(
+                "gather", ("z", d, n), allr.at[0, own, mine], allr.at[d, own, mine], z_peer(d)
+            )
     send("gather", ("core", 0), allr.at[0, own], allr.at[0, block(0, 1)], core_peer)
     send("gather", ("x", 0), allr.at[0, own], allr.at[0, beside], x_peer)
 
-    def from_z(d):
+    def from_z(d, n):
+        mine = cols(tp, n)
         view = allr.at[d, own, mine]
-        taken(view, at(("z", d)))
-        send("gather", ("x", d), view, allr.at[d, beside, mine], x_peer)
-        send("gather", ("y", d), view, view, y_peer)
+        taken(view, at(("z", d, n)))
+        send("gather", ("x", d, n), view, allr.at[d, beside, mine], x_peer)
+        send("gather", ("y", d, n), view, view, y_peer)
         send("gather", ("core", d), view, allr.at[d, block(0, 1), mine], core_peer)
 
-    def from_x(d):
-        view = allr.at[d, beside, mine] if d else allr.at[0, beside]
-        taken(view, at(("x", d)))
-        if d:
-            send("gather", ("y", d), view, view, y_peer)
-            send("gather", ("core", d), view, allr.at[d, block(1, 1), mine], core_peer)
-        else:
-            send("gather", ("core", 0), view, allr.at[0, block(1, 1)], core_peer)
+    def from_x(d, n):
+        mine = cols(tp, n)
+        view = allr.at[d, beside, mine]
+        taken(view, at(("x", d, n)))
+        send("gather", ("y", d, n), view, view, y_peer)
+        send("gather", ("core", d), view, allr.at[d, block(1, 1), mine], core_peer)
+
+    def from_beside():
+        view = allr.at[0, beside]
+        taken(view, at(("x", 0)))
+        send("gather", ("core", 0), view, allr.at[0, block(1, 1)], core_peer)
 
     def from_y(d):
-        view = allr.at[d, upper, other]
-        taken(view, at(("y", d)))
-        send("gather", ("core", d), view, allr.at[d, lower, other], core_peer)
-
-    lane = lax.broadcasted_iota(jnp.int32, (4 * rows, wall.shape[1]), 1)
+        for n in range(2):
+            view = allr.at[d, upper, cols(1 - tp, n)]
+            taken(view, at(("y", d, n)))
+            send("gather", ("core", d), view, allr.at[d, lower, cols(1 - tp, n)], core_peer)
+
+    square = lax.broadcasted_iota(jnp.int32, (rows, rows), 0) == lax.broadcasted_iota(
+        jnp.int32, (rows, rows), 1
+    )
+
+    def column(n):
+        return jnp.sum(jnp.where(square, wall[n, :, 0:rows], 0.0), axis=1, keepdims=True)
 
     def expert(d):
         taken(allr.at[d, lower], at(("core", d)))
@@ -142,8 +155,7 @@
         gate = jnp.dot(left, eg[...], preferred_element_type=F32)
         up = jnp.dot(left, eu[...], preferred_element_type=F32)
         hidden = ((gate / (1.0 + jnp.exp(-gate))) * up).astype(BF16)
-        marks = wall[d * 4 * rows : (d + 1) * 4 * rows, :]
-        weight = jnp.sum(jnp.where(lane == z, marks, 0.0), axis=1, keepdims=True)
+        weight = jnp.concatenate([column(4 * d + n) for n in range(4)], axis=0)
         for n in range(width // quarter):
             cols = slice(n * quarter, (n + 1) * quarter)
             prod[d, :, cols] = (
@@ -188,13 +200,16 @@
         outz[d, :, quarter:half] = high.astype(BF16)
         send("combine", "rz", outz.at[d], gotz.at[d], z_peer(d))
 
-    from_z(1)
-    from_x(0)
+    for n in range(2):
+        from_z(1, n)
+    from_beside()
     for d in range(2, zs):
-        from_z(d)
-        from_x(d - 1)
+        for n in range(2):
+            from_z(d, n)
+            from_x(d - 1, n)
     weights_here()
-    from_x(zs - 1)
+    for n in range(2):
+        from_x(zs - 1, n)
     from_y(1)
     expert(0)
     for d in range(1, zs):
@@ -203,8 +218,8 @@
         expert(d)
         if d > 1:
             first_sums(d - 1)
+    first_sums(zs - 1)
     second_sums(1)
-    first_sums(zs - 1)
     for d in range(2, zs):
         second_sums(d)
         if d == 2:
@@ -311,8 +326,15 @@
         assert number < limit
         return sem.at[number]
 
+    def across_z(d):
+        there = z
+        for step in range(zs.bit_length()):
+            if (d >> step) & 1:
+                there = there + (1 << step) * (1 - 2 * ((z // (1 << step)) % 2))
+        return there
+
     def z_peer(d):
-        return (((z + d + zs) % zs) * SPAN + place, tp)
+        return (across_z(d) * SPAN + place, tp)
 
     rows, width = tok.shape
     depth = wq_hbm.shape[0]
@@ -346,7 +368,7 @@
 
     def other(d, rx, rc):
         there = place + rc * (1 - 2 * (me % 2)) + rx * (2 - 4 * ((me // 2) % 2))
-        return (((z - d + zs) % zs) * SPAN + there, tp)
+        return (across_z(d) * SPAN + there, tp)
 
     partners = [other(*key) for key in others] + [y_peer]
     barrier = pltpu.get_barrier_semaphore()
@@ -391,21 +413,15 @@
 
     taken(routes, at("routes"))
     taken(shares, at("shares"))
-    square = lax.broadcasted_iota(jnp.int32, (rows, rows), 0) == lax.broadcasted_iota(
-        jnp.int32, (rows, rows), 1
-    )
-    mark_lane = lax.broadcasted_iota(jnp.int32, marks.shape, 1)
-    value = jnp.zeros(marks.shape, F32)
     for e in range(zs):
         line = jnp.sum(jnp.where(routes[...] == e, shares[...], 0.0), axis=0, keepdims=True)
-        column = jnp.sum(jnp.where(square, line, 0.0), axis=1, keepdims=True)
-        value = jnp.where(mark_lane == e, column, value)
-    marks[...] = value
-    wall[0:rows, :] = value
+        marks[e, :, 0:rows] = line
     for key in others:
         d, rx, rc = key
-        there = pl.ds(d * 4 * rows + rc * 2 * rows + rx * rows, rows)
-        remote(marks, wall.at[there], at("tags"), at("tag"), other(*key)).start()
+        there = other(*key)
+        slot = wall.at[d * 4 + rc * 2 + rx]
+        remote(marks.at[there[0] // SPAN], slot, at("tags"), at("tag"), there).start()
+    wall[0] = marks[z]
 
     def relay(k):
         view = weights.at[k, xs_rows]
@@ -419,7 +435,7 @@
         acc[k] = product[rows:].astype(BF16)
         for d in range(1, zs):
             view = pl.ds((d - 1) * rows, rows)
-            remote(acc.at[k, view], got.at[k, view], at("sums"), at(("sum", k)), z_peer(-d)).start()
+            remote(acc.at[k, view], got.at[k, view], at("sums"), at(("sum", k)), z_peer(d)).start()
 
     relay(order[0])
     relay(order[1])
@@ -456,7 +472,7 @@
             qs[kv, pl.ds(head, rows, stride=group), :] = block
             qs[kv, pl.ds(head + 1, rows, stride=group), :] = pltpu.roll(block, HEAD_DIM, 1)
 
-    unroll = 8
+    unroll = 16
     turns = rows // unroll
     span_len = cum.shape[2]
     places = lax.broadcasted_iota(jnp.int32, (group, span_len), 1)
@@ -562,7 +578,7 @@
     residual = tok[...].astype(F32) + normalized(mix) * gains[0]
     mixed_res[...] = residual
     allr[0, 0:rows, :] = (normalized(residual) * gains[1]).astype(BF16)
-    tagged = wall.at[pl.ds(rows, (4 * zs - 1) * rows)]
+    tagged = wall.at[pl.ds(1, 4 * zs - 1)]
     taken(tagged, at("tag"))
 
     def weights_here():
@@ -686,7 +702,9 @@
         and devices % SPAN == 0
         and key_cols == 2 * HEAD_DIM
         and 2 * key_cols == chunk
-        and row_count % 8 == 0
+        and row_count % 32 == 0
+        and row_count <= cache_keys.shape[1]
+        and model_width <= 2 * cache_keys.shape[2]
         and model_width % (2 * chunk) == 0
     )
     if dense:
@@ -695,7 +713,7 @@
         chunks = joint_cols // chunk
         heads_here = query_cols // HEAD_DIM
         strips = row_count * heads_here // 2
-        sems = 31 + 3 * chunks + 9 * zs
+        sems = 28 + 3 * chunks + 12 * zs
         smem = pltpu.SMEM
         half = model_width // 2
         layer_out, new_keys, new_values, gate_rows = communicate(
@@ -741,9 +759,9 @@
                 dma((sems,)),
                 VMEM((TOP, row_count), jnp.int32),
                 VMEM((TOP, row_count), F32),
-                VMEM((row_count, 128), F32),
+                VMEM((zs, 1, 128), F32),
                 VMEM((zs, SPAN * row_count, model_width), BF16),
-                VMEM((zs * SPAN * row_count, 128), F32),
+                VMEM((zs * SPAN, 1, 128), F32),
                 VMEM(expert_gate.shape, BF16),
                 VMEM(expert_up.shape, BF16),
                 VMEM(expert_down.shape, BF16),

time: 64.9 us -> 61.9 us (0.954)
  Pallas kernels: 64 us -> 61.1 us
    pallas_call x1, Pallas kernels: 62.5 us -> 59.5 us  [communicate(): pl.pallas_call(kernel, out_shape=out_shape, in_specs=[place] * len(operan...]
where the time goes in v4:
time: 61.9 us; the launch traced here: 61.7 us
  Pallas kernels  61.1 us (99%)
  between operations  0.65 us (1%)
    pallas_call x1, Pallas kernels, communicate(): pl.pallas_call(kernel, out_shape=out_shape, in_specs=[place] * len(operan...  59.5 us
    pallas_call x1, Pallas kernels, deliver(): pl.pallas_call(functools.partial(deliver_kernel, count), out_shape=tuple(...  1.55 us

profile of v4, /device:TPU:0, one launch (start us, length us, event | category | flops | bytes accessed | tf_op | source)
XLA Modules:
  0.0 61.7 jit_solution(2739633024308548771)
XLA Ops:
  0.6 59.5 %shard_map.210 = (bf16[32,1024]{1,0:T(8,128)(2,1)}, bf16[32,128]{1,0:T(8,128)(2,1)}, bf16[32,128]{1,0:T(8,128)(2,1)}, f32[16,32]{1,0:T(8,128)}) custom-call(bf16[32,2048]{1,0:T(8,128)(2,1)} %tok_hbm.1, f32[1,2048]{1,0:T(1,128)} %bitcast.8, bf16[128,1024]{1,0:T(8,128)(2,1)} %wq_hbm.1, bf16[128,128]{1,0:T(8,128)(2,1)} %wk_hbm.1, bf16[128,128]{1,0:T(8,128)(2,1)} %wv_hbm.1, ...), custom_call_target="tpu_custom_call" | custom-call | tf_op jit(solution)/shard_map/pallas_call | solution.py:623
  60.2 1.5 %shard_map.211 = (bf16[32,1024]{1,0:T(8,128)(2,1)}, bf16[32,128]{1,0:T(8,128)(2,1)}, bf16[32,128]{1,0:T(8,128)(2,1)}, f32[16,32]{1,0:T(8,128)}) custom-call(bf16[32,1024]{1,0:T(8,128)(2,1)} %get-tuple-element.12.refs_0_, bf16[32,128]{1,0:T(8,128)(2,1)} %get-tuple-element.13.refs_1_, bf16[32,128]{1,0:T(8,128)(2,1)} %get-tuple-element.14.refs_2_, ...), custom_call_target="tpu_custom_call" | custom-call | tf_op jit(solution)/shard_map/pallas_call | solution.py:652

commit v5 on v4

--- a/solution.py
+++ b/solution.py
@@ -438,13 +438,12 @@
             remote(acc.at[k, view], got.at[k, view], at("sums"), at(("sum", k)), z_peer(d)).start()
 
     relay(order[0])
-    relay(order[1])
     taken(xs.at[pl.ds(rows, (zs - 1) * rows)], at("slab"))
     taken(view, at("direct"))
     for n, k in enumerate(order):
+        if n + 1 < chunks:
+            relay(order[n + 1])
         multiply(k)
-        if n + 2 < chunks:
-            relay(order[n + 2])
 
     lane = lax.broadcasted_iota(jnp.int32, (rows, 2 * HEAD_DIM), 1)
     low = lane < HEAD_DIM

time: 61.9 us -> 62 us (level)
  no operation moved by 1% of the time
where the time goes in v5:
time: 62 us; the launch traced here: 61.8 us
  Pallas kernels  61.2 us (99%)
  between operations  0.65 us (1%)
    pallas_call x1, Pallas kernels, communicate(): pl.pallas_call(kernel, out_shape=out_shape, in_specs=[place] * len(operan...  59.6 us
    pallas_call x1, Pallas kernels, deliver(): pl.pallas_call(functools.partial(deliver_kernel, count), out_shape=tuple(...  1.55 us

profile of v5, /device:TPU:0, one launch (start us, length us, event | category | flops | bytes accessed | tf_op | source)
XLA Modules:
  0.0 61.8 jit_solution(12124236433380397929)
XLA Ops:
  0.6 59.6 %shard_map.210 = (bf16[32,1024]{1,0:T(8,128)(2,1)}, bf16[32,128]{1,0:T(8,128)(2,1)}, bf16[32,128]{1,0:T(8,128)(2,1)}, f32[16,32]{1,0:T(8,128)}) custom-call(bf16[32,2048]{1,0:T(8,128)(2,1)} %tok_hbm.1, f32[1,2048]{1,0:T(1,128)} %bitcast.8, bf16[128,1024]{1,0:T(8,128)(2,1)} %wq_hbm.1, bf16[128,128]{1,0:T(8,128)(2,1)} %wk_hbm.1, bf16[128,128]{1,0:T(8,128)(2,1)} %wv_hbm.1, ...), custom_call_target="tpu_custom_call" | custom-call | tf_op jit(solution)/shard_map/pallas_call | solution.py:622
  60.3 1.5 %shard_map.211 = (bf16[32,1024]{1,0:T(8,128)(2,1)}, bf16[32,128]{1,0:T(8,128)(2,1)}, bf16[32,128]{1,0:T(8,128)(2,1)}, f32[16,32]{1,0:T(8,128)}) custom-call(bf16[32,1024]{1,0:T(8,128)(2,1)} %get-tuple-element.12.refs_0_, bf16[32,128]{1,0:T(8,128)(2,1)} %get-tuple-element.13.refs_1_, bf16[32,128]{1,0:T(8,128)(2,1)} %get-tuple-element.14.refs_2_, ...), custom_call_target="tpu_custom_call" | custom-call | tf_op jit(solution)/shard_map/pallas_call | solution.py:651
